TPU v7x, 32 devices: a whole 2x2x4 slice. The times are simulated.
32 devices in a mesh: sp: 8 (over z, x), tp: 4 (over y, core).
Axes of the slice: x: 2, y: 2, z: 4, core: 2. Of those that a mesh axis runs over, the one named last changes fastest.
Arguments:
- out_cotangent: bfloat16 [2048, 2048], P('sp'), may hold values from -6 to 6
- stream: bfloat16 [2048, 2048], P('sp'), may hold values from -6 to 6
- route_ids: int32 [2048, 2], P('sp'), may hold values from 0 to 7, all different within a row; in each aligned block of 256 rows (0 to 255, 256 to 511, ...) at most 128 rows name the same one
- route_weights: float32 [2048, 2], P('sp'), may hold values from 0.3 to 2
- gate_proj: bfloat16 [8, 2048, 1024], P('sp', None, 'tp'), may hold values from -0.125 to 0.125
- up_proj: bfloat16 [8, 2048, 1024], P('sp', None, 'tp'), may hold values from -0.125 to 0.125
- down_proj: bfloat16 [8, 1024, 2048], P('sp', 'tp'), may hold values from -0.1875 to 0.1875
- outer_gate: bfloat16 [2048, 512], P('sp', 'tp'), may hold values from -6 to 6
- inner_gate: bfloat16 [2048, 512], P('sp', 'tp'), may hold values from -6 to 6
- conv_input: bfloat16 [2048, 512], P('sp', 'tp'), may hold values from -6 to 6
- conv_taps: float32 [3, 512], P(None, 'tp'), may hold values from -4 to 4
- out_proj: bfloat16 [2048, 512], P(None, 'tp'), may hold values from -0.25 to 0.25
Outputs:
- grad_gate_proj: bfloat16 [8, 2048, 1024], P('sp', None, 'tp')
- grad_up_proj: bfloat16 [8, 2048, 1024], P('sp', None, 'tp')
- grad_down_proj: bfloat16 [8, 1024, 2048], P('sp', 'tp')
- grad_out_proj: float32 [2048, 512], P('sp', 'tp')
- grad_outer_gate: float32 [2048, 512], P('sp', 'tp')
- grad_inner_gate: float32 [2048, 512], P('sp', 'tp')
- grad_conv_input: float32 [2048, 512], P('sp', 'tp')
Inputs may be any that keep to these rules, and one draw needn't show every extreme that they name: `route_ids`: the 2 experts of a token differ. Among the tokens of one index of sp, no expert is chosen more than 128 times, and in every draw some expert is chosen exactly 128 times by them.
All inputs are finite; a program needn't handle non-finite values.
Results may differ from a plain program's by a relative error of at most 0.018.
Values may be sent and summed in bfloat16 or wider, within the bound.
A program may use at most 64 MiB of HBM per device.

v0:
```python
import jax
import jax.numpy as jnp
from jax import lax
from jax.sharding import PartitionSpec as P


def passed_along(x, axis, by):
    devices = lax.axis_size(axis)
    pairs = [(i, i + by) for i in range(devices) if 0 <= i + by < devices]
    return lax.ppermute(x, axis, pairs)


def shards(
    out_cotangent,
    stream,
    route_ids,
    route_weights,
    gate_proj,
    up_proj,
    down_proj,
    outer_gate,
    inner_gate,
    conv_input,
    conv_taps,
    out_proj,
):
    sp_devices = lax.axis_size("sp")
    tokens_here, width = stream.shape
    choices_each = route_ids.shape[1]
    experts = sp_devices * gate_proj.shape[0]
    capacity = 4 * tokens_here // experts
    assigned = tokens_here * choices_each
    flat_expert = route_ids.reshape(-1)
    onehot = (flat_expert[:, None] == jnp.arange(experts, dtype=jnp.int32)[None, :]).astype(
        jnp.int32
    )
    earlier_count = jnp.cumsum(onehot, axis=0) - onehot
    slot_rank = jnp.sum(earlier_count * onehot, axis=1)
    destination = flat_expert * capacity + slot_rank
    slot_source = (
        jnp.full((experts * capacity,), assigned, jnp.int32)
        .at[destination]
        .set(jnp.arange(assigned, dtype=jnp.int32))
    )
    token_of = jnp.arange(assigned, dtype=jnp.int32) // choices_each
    scaled = (
        route_weights.reshape(-1)[:, None] * out_cotangent[token_of].astype(jnp.float32)
    ).astype(jnp.bfloat16)
    zero_row = jnp.zeros((1, width), jnp.bfloat16)
    send_grad = jnp.concatenate([scaled, zero_row], axis=0)[slot_source].reshape(
        sp_devices, capacity, width
    )
    slot_token = jnp.where(slot_source < assigned, slot_source // choices_each, tokens_here)
    send_input = jnp.concatenate([stream, zero_row], axis=0)[slot_token].reshape(
        sp_devices, capacity, width
    )
    got_grad, got_input = (
        lax.all_to_all(send_grad, "sp", split_axis=0, concat_axis=0, tiled=True),
        lax.all_to_all(send_input, "sp", split_axis=0, concat_axis=0, tiled=True),
    )
    rows_grad = got_grad.reshape(-1, width)
    rows_input = got_input.reshape(-1, width)
    w_gate = gate_proj[0]
    w_up = up_proj[0]
    w_down = down_proj[0]
    gate = jnp.dot(rows_input, w_gate, preferred_element_type=jnp.float32)
    up = jnp.dot(rows_input, w_up, preferred_element_type=jnp.float32)
    sig = jax.nn.sigmoid(gate)
    silu_gate = gate * sig
    hidden = (silu_gate * up).astype(jnp.bfloat16)
    across = (((1,), (1,)), ((), ()))
    d_hidden = lax.dot_general(rows_grad, w_down, across, preferred_element_type=jnp.float32)
    d_gate = (d_hidden * up * sig * (1.0 + gate * (1.0 - sig))).astype(jnp.bfloat16)
    d_up = (d_hidden * silu_gate).astype(jnp.bfloat16)
    over_rows = (((0,), (0,)), ((), ()))
    grad_down = lax.dot_general(
        hidden, rows_grad, over_rows, preferred_element_type=jnp.float32
    ).astype(jnp.bfloat16)
    grad_gate = lax.dot_general(
        rows_input, d_gate, over_rows, preferred_element_type=jnp.float32
    ).astype(jnp.bfloat16)
    grad_up = lax.dot_general(
        rows_input, d_up, over_rows, preferred_element_type=jnp.float32
    ).astype(jnp.bfloat16)
    partial_input = lax.dot_general(
        d_gate, w_gate, across, preferred_element_type=jnp.float32
    ) + lax.dot_general(d_up, w_up, across, preferred_element_type=jnp.float32)
    share = lax.psum_scatter(
        partial_input.astype(jnp.bfloat16), "tp", scatter_dimension=1, tiled=True
    )
    quarter = share.shape[1]
    returned = lax.all_to_all(
        share.reshape(sp_devices, capacity, quarter), "sp", split_axis=0, concat_axis=0, tiled=True
    )
    per_assigned = returned.reshape(-1, quarter)[destination].astype(jnp.float32)
    moe_grad = jnp.sum(per_assigned.reshape(tokens_here, choices_each, quarter), axis=1)
    own_cotangent = lax.dynamic_slice_in_dim(
        out_cotangent, lax.axis_index("tp") * quarter, quarter, 1
    )
    stream_part = (own_cotangent.astype(jnp.float32) + moe_grad).astype(jnp.bfloat16)
    stream_grad = lax.all_gather(stream_part, "tp", axis=1, tiled=True)
    mixed = inner_gate.astype(jnp.float32) * conv_input.astype(jnp.float32)
    previous = passed_along(mixed[tokens_here - 2 :], "sp", 1)
    extended = jnp.concatenate([previous, mixed], axis=0)
    conv_out = (
        conv_taps[0] * extended[:tokens_here]
        + conv_taps[1] * extended[1 : tokens_here + 1]
        + conv_taps[2] * extended[2:]
    )
    mixer_out = (outer_gate.astype(jnp.float32) * conv_out).astype(jnp.bfloat16)
    d_mixer = jnp.dot(stream_grad, out_proj, preferred_element_type=jnp.float32)
    grad_outer = d_mixer * conv_out
    d_conv = d_mixer * outer_gate.astype(jnp.float32)
    following = passed_along(d_conv[:2], "sp", -1)
    trailing = jnp.concatenate([d_conv, following], axis=0)
    d_mixed = (
        conv_taps[2] * trailing[:tokens_here]
        + conv_taps[1] * trailing[1 : tokens_here + 1]
        + conv_taps[0] * trailing[2:]
    )
    grad_inner = d_mixed * conv_input.astype(jnp.float32)
    grad_input = d_mixed * inner_gate.astype(jnp.float32)
    grad_projection = lax.psum_scatter(
        lax.dot_general(stream_grad, mixer_out, over_rows, preferred_element_type=jnp.float32),
        "sp",
        scatter_dimension=0,
        tiled=True,
    )
    return (
        grad_gate[None],
        grad_up[None],
        grad_down[None],
        grad_projection,
        grad_outer,
        grad_inner,
        grad_input,
    )


def solution(mesh):
    placed = (
        P("sp", None),
        P("sp", None),
        P("sp", None),
        P("sp", None),
        P("sp", None, "tp"),
        P("sp", None, "tp"),
        P("sp", "tp", None),
        P("sp", "tp"),
        P("sp", "tp"),
        P("sp", "tp"),
        P(None, "tp"),
        P(None, "tp"),
    )
    return jax.shard_map(
        shards,
        mesh=mesh,
        in_specs=placed,
        out_specs=(
            P("sp", None, "tp"),
            P("sp", None, "tp"),
            P("sp", "tp", None),
            P("sp", "tp"),
            P("sp", "tp"),
            P("sp", "tp"),
            P("sp", "tp"),
        ),
        check_vma=False,
    )
```

profile of v0, /device:TPU:0, one launch (start us, length us, event | category | flops | bytes accessed | tf_op | source)
XLA Modules:
  0.0 399.2 jit_solution(9364566062263864789)
XLA Ops:
  7.2 0.8 broadcast_multiply_fusion
  8.0 0.8 copy.20
  8.8 0.1 eq.29
  8.9 0.1 eq.25
  9.1 0.1 copy.19
  9.2 0.1 mul.121
  9.4 1.1 reduce-window.6
  10.5 0.2 slice_reduce_fusion
  10.8 0.1 fusion.28
  10.9 2.4 scatter_custom_fusion
  13.4 1.3 concatenate.12
  14.7 6.1 %gather_fusion = bf16[1024,2048]{1,0:T(8,128)(2,1)} fusion(bf16[257,2048]{1,0:T(8,128)(2,1)S(1)} %concatenate.12, s32[1024]{0:T(1024)S(1)} %get-tuple-element.15), kind=kCustom, calls=%fused_computation | custom fusion | bytes 8392704 | tf_op jit(solution)/shard_map/gather | solution.py:54
  20.8 7.4 %all-to-all-start = ((bf16[8,128,2048]{2,1,0:T(8,128)(2,1)}), bf16[8,128,2048]{2,1,0:T(8,128)(2,1)}, u32[]{:S(2)}, u32[]{:S(2)}) async-start(bf16[8,128,2048]{2,1,0:T(8,128)(2,1)} %bitcast.58), calls=%async_computation | async-start | bytes 8388608 | tf_op jit(solution)/shard_map/all_to_all | solution.py:59
  28.2 0.1 copy.22
  28.3 0.1 mul.123
  28.5 3.3 gather_fusion.1
  31.8 2.0 multiply_convert_fusion
  33.8 0.2 concatenate.13
  34.0 6.0 %gather_fusion.2 = bf16[1024,2048]{1,0:T(8,128)(2,1)} fusion(bf16[513,2048]{1,0:T(8,128)(2,1)S(1)} %concatenate.13, s32[1024]{0:T(1024)S(1)} %get-tuple-element.14), kind=kCustom, calls=%fused_computation.2 | custom fusion | bytes 8392704 | tf_op jit(solution)/shard_map/gather | solution.py:50
  40.0 81.4 %all-to-all-done = bf16[8,128,2048]{2,1,0:T(8,128)(2,1)} async-done(((bf16[8,128,2048]{2,1,0:T(8,128)(2,1)}), bf16[8,128,2048]{2,1,0:T(8,128)(2,1)}, u32[]{:S(2)}, u32[]{:S(2)}) %all-to-all-start) | async-done | bytes 4194336 | tf_op jit(solution)/shard_map/all_to_all | solution.py:59
  121.5 4.6 %all-to-all-start.1 = ((bf16[8,128,2048]{2,1,0:T(8,128)(2,1)}), bf16[8,128,2048]{2,1,0:T(8,128)(2,1)}, u32[]{:S(2)}, u32[]{:S(2)}) async-start(bf16[8,128,2048]{2,1,0:T(8,128)(2,1)} %bitcast.59), calls=%async_computation.1 | async-start | bytes 8388608 | tf_op jit(solution)/shard_map/all_to_all | solution.py:58
  126.0 0.0 reduce-scatter.3.cloned.1.call-start
  126.1 4.5 %fusion.5 = f32[1024,256]{1,0:T(8,128)} fusion(bf16[1024,2048]{1,0:T(8,128)(2,1)} %bitcast.5, bf16[1,2048,256]{2,1,0:T(8,128)(2,1)S(1)} %copy-done), kind=kOutput, calls=%fused_computation.15 | convolution fusion | flops 1073741824 | bytes 6291456 | tf_op jit(solution)/shard_map/dot_general | solution.py:66
  130.6 4.4 %fusion.8 = f32[1024,256]{1,0:T(8,128)} fusion(bf16[1024,2048]{1,0:T(8,128)(2,1)} %bitcast.5, bf16[1,2048,256]{2,1,0:T(8,128)(2,1)S(1)} %copy-done.2), kind=kOutput, calls=%fused_computation.18 | convolution fusion | flops 1073741824 | bytes 6291456 | tf_op jit(solution)/shard_map/dot_general | solution.py:67
  135.0 83.6 %all-to-all-done.1 = bf16[8,128,2048]{2,1,0:T(8,128)(2,1)} async-done(((bf16[8,128,2048]{2,1,0:T(8,128)(2,1)}), bf16[8,128,2048]{2,1,0:T(8,128)(2,1)}, u32[]{:S(2)}, u32[]{:S(2)}) %all-to-all-start.1) | async-done | bytes 4194336 | tf_op jit(solution)/shard_map/all_to_all | solution.py:58
  218.6 4.6 %multiply_convert_fusion.2 = (bf16[1024,256]{1,0:T(8,128)(2,1)S(1)}, bf16[1024,256]{1,0:T(8,128)(2,1)S(1)}) fusion(f32[1024,256]{1,0:T(8,128)} %fusion.5, f32[1024,256]{1,0:T(8,128)} %fusion.8, bf16[1024,2048]{1,0:T(8,128)(2,1)} %bitcast.8, bf16[1,256,2048]{2,1,0:T(8,128)(2,1)} %param.18), kind=kOutput, calls=%fused_computation.23 | convolution fusion | flops 1077149696 | bytes 8388608 | tf_op jit(solution)/shard_map/dot_general | solution.py:72
  223.2 1.3 fusion.3
  224.5 3.4 add_convert_fusion
  227.9 43.6 %reduce-scatter.3.cloned.1.call-done = bf16[1024,512]{1,0:T(8,128)(2,1)} async-done(((bf16[1024,2048]{1,0:T(8,128)(2,1)}), bf16[1024,512]{1,0:T(8,128)(2,1)}) %reduce-scatter.3.cloned.1.call-update) | async-done | bytes 1048592 | tf_op jit(solution)/shard_map/reduce_scatter | solution.py:88
  271.5 5.5 %all-to-all-start.2 = ((bf16[8,128,512]{2,1,0:T(8,128)(2,1)}), bf16[8,128,512]{2,1,0:T(8,128)(2,1)S(1)}, u32[]{:S(2)}, u32[]{:S(2)}) async-start(bf16[8,128,512]{2,1,0:T(8,128)(2,1)} %bitcast.60), calls=%async_computation.3 | async-start | bytes 2097152 | tf_op jit(solution)/shard_map/all_to_all | solution.py:92
  277.0 0.2 all-gather.2.cloned.1.call-start
  277.3 25.4 %all-to-all-done.2 = bf16[8,128,512]{2,1,0:T(8,128)(2,1)S(1)} async-done(((bf16[8,128,512]{2,1,0:T(8,128)(2,1)}), bf16[8,128,512]{2,1,0:T(8,128)(2,1)S(1)}, u32[]{:S(2)}, u32[]{:S(2)}) %all-to-all-start.2) | async-done | bytes 1048608 | tf_op jit(solution)/shard_map/all_to_all | solution.py:92
  302.7 2.0 gather_fusion.3
  304.7 0.7 reshape.133
  305.3 1.2 reduce_sum.22
  306.6 1.7 add_convert_fusion.1
  308.4 3.3 collective-permute-start
  311.7 1.3 collective-permute-done
  313.0 10.2 %all-gather.2.cloned.1.call-done = bf16[256,2048]{1,0:T(8,128)(2,1)} async-done(((bf16[256,512]{1,0:T(8,128)(2,1)}), bf16[256,2048]{1,0:T(8,128)(2,1)}) %all-gather.2.cloned.1.call-update) | async-done | bytes 1048592 | tf_op jit(solution)/shard_map/all_gather | solution.py:101
  323.2 2.4 fusion.39
  325.7 2.8 fusion.25
  328.5 4.6 %fusion = bf16[1,2048,256]{2,1,0:T(8,128)(2,1)} fusion(bf16[1024,2048]{1,0:T(8,128)(2,1)} %bitcast.5, bf16[1024,256]{1,0:T(8,128)(2,1)S(1)} %get-tuple-element.12), kind=kOutput, calls=%fused_computation.10 | convolution fusion | flops 1074266112 | bytes 5767168 | tf_op jit(solution)/shard_map/dot_general | solution.py:79
  333.1 4.6 %fusion.2 = bf16[1,256,2048]{2,1,0:T(8,128)(2,1)} fusion(bf16[1024,2048]{1,0:T(8,128)(2,1)} %bitcast.8, f32[1024,256]{1,0:T(8,128)S(1)} %copy-done.11, f32[1024,256]{1,0:T(8,128)S(1)} %copy-done.10), kind=kOutput, calls=%fused_computation.12 | convolution fusion | flops 1075838976 | bytes 7340032 | tf_op jit(solution)/shard_map/dot_general | solution.py:76
  337.7 1.3 collective-permute-start.1
  339.0 4.5 %fusion.1 = bf16[1,2048,256]{2,1,0:T(8,128)(2,1)} fusion(bf16[1024,2048]{1,0:T(8,128)(2,1)} %bitcast.5, bf16[1024,256]{1,0:T(8,128)(2,1)S(1)} %copy-done.4), kind=kOutput, calls=%fused_computation.11 | convolution fusion | flops 1074266112 | bytes 5767168 | tf_op jit(solution)/shard_map/dot_general | solution.py:82
  343.6 0.7 convert_multiply_fusion.2
  344.3 0.7 convert_multiply_fusion
  344.9 47.8 %reduce-scatter.5.cloned.1.call-done = f32[256,128]{1,0:T(8,128)} async-done(((f32[2048,128]{1,0:T(8,128)}), f32[256,128]{1,0:T(8,128)}) %reduce-scatter.5.cloned.1.call-update) | async-done | bytes 131088 | tf_op jit(solution)/shard_map/reduce_scatter | solution.py:123
  (42 shorter events, 0.3 us)
Async XLA Ops:
  7.2 118.9 %copy-start = (bf16[1,2048,256]{2,1,0:T(8,128)(2,1)S(1)}, bf16[1,2048,256]{2,1,0:T(8,128)(2,1)}, u32[]{:S(2)}) copy-start(bf16[1,2048,256]{2,1,0:T(8,128)(2,1)} %param.16) | copy-start | bytes 3145732
  20.8 7.4 %copy-start.8 = (f32[256,2]{0,1:T(2,128)S(1)}, f32[256,2]{0,1:T(2,128)}, u32[]{:S(2)}) copy-start(f32[256,2]{0,1:T(2,128)} %param.15) | copy-start | bytes 6148
  20.8 7.7 %copy-start.1 = (bf16[256,2048]{1,0:T(8,128)(2,1)S(1)}, bf16[256,2048]{1,0:T(8,128)(2,1)}, u32[]{:S(2)}) copy-start(bf16[256,2048]{1,0:T(8,128)(2,1)} %param.12) | copy-start | bytes 3145732
  20.8 100.7 %all-to-all-start = ((bf16[8,128,2048]{2,1,0:T(8,128)(2,1)}), bf16[8,128,2048]{2,1,0:T(8,128)(2,1)}, u32[]{:S(2)}, u32[]{:S(2)}) async-start(bf16[8,128,2048]{2,1,0:T(8,128)(2,1)} %bitcast.58), calls=%async_computation | async-start | bytes 8388608 | tf_op jit(solution)/shard_map/all_to_all | solution.py:59
  121.5 97.1 %all-to-all-start.1 = ((bf16[8,128,2048]{2,1,0:T(8,128)(2,1)}), bf16[8,128,2048]{2,1,0:T(8,128)(2,1)}, u32[]{:S(2)}, u32[]{:S(2)}) async-start(bf16[8,128,2048]{2,1,0:T(8,128)(2,1)} %bitcast.59), calls=%async_computation.1 | async-start | bytes 8388608 | tf_op jit(solution)/shard_map/all_to_all | solution.py:58
  126.0 4.6 %copy-start.2 = (bf16[1,2048,256]{2,1,0:T(8,128)(2,1)S(1)}, bf16[1,2048,256]{2,1,0:T(8,128)(2,1)}, u32[]{:S(2)}) copy-start(bf16[1,2048,256]{2,1,0:T(8,128)(2,1)} %param.17) | copy-start | bytes 3145732
  126.0 145.5 %reduce-scatter.3.cloned.1.call-start = ((), (), s32[]{:S(2)}) async-start(), calls=%async_computation.5 | async-start | bytes 5242880 | tf_op jit(solution)/shard_map/reduce_scatter | solution.py:88
  223.2 1.3 copy-start.3
  271.5 31.2 %all-to-all-start.2 = ((bf16[8,128,512]{2,1,0:T(8,128)(2,1)}), bf16[8,128,512]{2,1,0:T(8,128)(2,1)S(1)}, u32[]{:S(2)}, u32[]{:S(2)}) async-start(bf16[8,128,512]{2,1,0:T(8,128)(2,1)} %bitcast.60), calls=%async_computation.3 | async-start | bytes 2097152 | tf_op jit(solution)/shard_map/all_to_all | solution.py:92
  277.0 46.2 %all-gather.2.cloned.1.call-start = ((), (), s32[]{:S(2)}) async-start(), calls=%async_computation.6 | async-start | bytes 1310720 | tf_op jit(solution)/shard_map/all_gather | solution.py:101
  302.7 5.7 %copy-start.6 = (bf16[256,128]{1,0:T(8,128)(2,1)S(1)}, bf16[256,128]{1,0:T(8,128)(2,1)}, u32[]{:S(2)}) copy-start(bf16[256,128]{1,0:T(8,128)(2,1)} %param.21) | copy-start | bytes 196612
  302.7 5.7 %copy-start.7 = (bf16[256,128]{1,0:T(8,128)(2,1)S(1)}, bf16[256,128]{1,0:T(8,128)(2,1)}, u32[]{:S(2)}) copy-start(bf16[256,128]{1,0:T(8,128)(2,1)} %param.20) | copy-start | bytes 196612
  302.7 9.0 %copy-start.9 = (f32[3,128]{1,0:T(4,128)S(1)}, f32[3,128]{1,0:T(4,128)}, u32[]{:S(2)}) copy-start(f32[3,128]{1,0:T(4,128)} %param.22) | copy-start | bytes 4612
  302.7 20.5 %copy-start.5 = (bf16[256,128]{1,0:T(8,128)(2,1)S(1)}, bf16[256,128]{1,0:T(8,128)(2,1)}, u32[]{:S(2)}) copy-start(bf16[256,128]{1,0:T(8,128)(2,1)} %param.19) | copy-start | bytes 196612
  308.3 84.4 %reduce-scatter.5.cloned.1.call-start = ((), (), s32[]{:S(2)}) async-start(), calls=%async_computation.7 | async-start | bytes 1179648 | tf_op jit(solution)/shard_map/reduce_scatter | solution.py:123
  308.4 4.6 %collective-permute-start = (f32[2,128]{1,0:T(2,128)S(1)}, f32[2,128]{1,0:T(2,128)S(1)}, u32[]{:S(2)}, u32[]{:S(2)}) collective-permute-start(f32[2,128]{1,0:T(2,128)S(1)} %slice.56), channel_id=1, source_target_pairs={{0,4},{4,8},{8,12},{12,16},{16,20},{20,24},{24,28},{1,5},{5,9},{9,... | collective-permute-start | bytes 3080 | tf_op jit(solution)/shard_map/ppermute | solution.py:10
  328.5 4.7 %copy-start.10 = (f32[1024,256]{1,0:T(8,128)S(1)}, f32[1024,256]{1,0:T(8,128)}, u32[]{:S(2)}) copy-start(f32[1024,256]{1,0:T(8,128)} %fusion.5) | copy-start | bytes 3145732
  328.5 4.6 %copy-start.11 = (f32[1024,256]{1,0:T(8,128)S(1)}, f32[1024,256]{1,0:T(8,128)}, u32[]{:S(2)}) copy-start(f32[1024,256]{1,0:T(8,128)} %fusion.8) | copy-start | bytes 3145732
  333.1 5.9 %copy-start.4 = (bf16[1024,256]{1,0:T(8,128)(2,1)S(1)}, bf16[1024,256]{1,0:T(8,128)(2,1)}, u32[]{:S(2)}) copy-start(bf16[1024,256]{1,0:T(8,128)(2,1)} %copy-done.3) | copy-start | bytes 1572868
  337.7 5.8 %collective-permute-start.1 = (f32[2,128]{1,0:T(2,128)S(1)}, f32[2,128]{1,0:T(2,128)S(1)}, u32[]{:S(2)}, u32[]{:S(2)}) collective-permute-start(f32[2,128]{1,0:T(2,128)S(1)} %slice.59), channel_id=1, source_target_pairs={{4,0},{8,4},{12,8},{16,12},{20,16},{24,20},{28,24},{5,1},{9,5},{13... | collective-permute-start | bytes 3080 | tf_op jit(solution)/shard_map/ppermute | solution.py:10
Sparse Core Ops, SparseCore 0:
  228.0 43.4 reduce-scatter.2
  308.5 14.7 all-gather.1
  328.6 64.0 reduce-scatter.4
where the time goes:
time: 400 us; the launch traced here: 399 us
  waiting for transfers between devices  293 us (73%)
  matrix products  37.1 us (9%)
  local copies, waits for them, and re-layouts  23.9 us (6%)
  starting transfers between devices  22.3 us (6%)
  between operations  14.1 us (4%)
  other arithmetic  8.45 us (2%)
    all_to_all x1, waiting for transfers between devices, shards(): lax.all_to_all(send_grad, 'sp', split_axis=0, concat_axis=0, tiled=True)  83.6 us
    all_to_all x1, waiting for transfers between devices, shards(): lax.all_to_all(send_input, 'sp', split_axis=0, concat_axis=0, tiled=True)  81.4 us
    reduce_scatter x1, waiting for transfers between devices, shards(): lax.psum_scatter(lax.dot_general(stream_grad, mixer_out, over_rows, prefe...  47.8 us
    reduce_scatter x1, waiting for transfers between devices, shards(): lax.psum_scatter(partial_input.astype(jnp.bfloat16), 'tp', scatter_dimens...  43.6 us
    all_to_all x1, waiting for transfers between devices, shards(): lax.all_to_all(share.reshape(sp_devices, capacity, quarter), 'sp', split_...  25.4 us
    all_gather x1, waiting for transfers between devices, shards(): stream_grad = lax.all_gather(stream_part, 'tp', axis=1, tiled=True)  10.2 us
  transfers between devices with their start and end apart: 8, of which 7 were waited for; matrix products, arithmetic and copies ran while one was open for 9% of the time, Pallas kernels for 0%

commit v1 on v0

v1 whole, which is shorter than its diff:
```python
import jax
import jax.numpy as jnp
from jax import lax
from jax.sharding import PartitionSpec as P


def passed_along(x, axis, by):
    devices = lax.axis_size(axis)
    pairs = [(i, i + by) for i in range(devices) if 0 <= i + by < devices]
    return lax.ppermute(x, axis, pairs)


def to_owners(x, devices):
    blocks = x.reshape(devices, -1, x.shape[1])
    return lax.all_to_all(blocks, "sp", split_axis=0, concat_axis=0, tiled=True).reshape(x.shape)


def shards(
    out_cotangent,
    stream,
    route_ids,
    route_weights,
    gate_proj,
    up_proj,
    down_proj,
    outer_gate,
    inner_gate,
    conv_input,
    conv_taps,
    out_proj,
):
    sp_devices = lax.axis_size("sp")
    tokens_here, width = stream.shape
    experts = sp_devices * gate_proj.shape[0]
    capacity = 4 * tokens_here // experts
    quarter = width // lax.axis_size("tp")
    first_column = lax.axis_index("tp") * quarter
    own_cotangent = lax.dynamic_slice_in_dim(out_cotangent, first_column, quarter, 1)
    own_stream = lax.dynamic_slice_in_dim(stream, first_column, quarter, 1)
    over_rows = (((0,), (0,)), ((), ()))
    expert_ids = jnp.arange(experts, dtype=jnp.int32)
    chosen = route_ids[:, :, None] == expert_ids
    hit = jnp.any(chosen, axis=1)
    token_weight = jnp.sum(jnp.where(chosen, route_weights[:, :, None], 0.0), axis=1)
    token_ids = jnp.arange(tokens_here, dtype=jnp.int32)
    below = (token_ids[:, None] < token_ids[None, :]).astype(jnp.bfloat16)
    rank = lax.dot_general(
        hit.astype(jnp.bfloat16), below, over_rows, preferred_element_type=jnp.float32
    )
    rank = jnp.where(hit.T, rank, -1.0)
    in_slot = rank[:, None, :] == jnp.arange(capacity, dtype=jnp.float32)[None, :, None]
    slot_weight = jnp.sum(jnp.where(in_slot, token_weight.T[:, None, :], 0.0), axis=2)
    pick = in_slot.astype(jnp.bfloat16).reshape(experts * capacity, tokens_here)
    send_input = jnp.dot(pick, own_stream, preferred_element_type=jnp.float32).astype(jnp.bfloat16)
    send_grad = (
        slot_weight.reshape(-1, 1)
        * jnp.dot(pick, own_cotangent, preferred_element_type=jnp.float32)
    ).astype(jnp.bfloat16)
    got_input = to_owners(send_input, sp_devices)
    rows_input = lax.all_gather(got_input, "tp", axis=1, tiled=True)
    send_grad, got_input = lax.optimization_barrier((send_grad, got_input))
    got_grad = to_owners(send_grad, sp_devices)
    rows_grad = lax.all_gather(got_grad, "tp", axis=1, tiled=True)
    mixed = inner_gate.astype(jnp.float32) * conv_input.astype(jnp.float32)
    previous = passed_along(mixed[tokens_here - 2 :], "sp", 1)
    extended = jnp.concatenate([previous, mixed], axis=0)
    conv_out = (
        conv_taps[0] * extended[:tokens_here]
        + conv_taps[1] * extended[1 : tokens_here + 1]
        + conv_taps[2] * extended[2:]
    )
    mixer_out = (outer_gate.astype(jnp.float32) * conv_out).astype(jnp.bfloat16)
    conv_out, mixer_out, rows_grad = lax.optimization_barrier((conv_out, mixer_out, rows_grad))
    w_gate = gate_proj[0]
    w_up = up_proj[0]
    w_down = down_proj[0]
    gate = jnp.dot(rows_input, w_gate, preferred_element_type=jnp.float32)
    up = jnp.dot(rows_input, w_up, preferred_element_type=jnp.float32)
    sig = jax.nn.sigmoid(gate)
    silu_gate = gate * sig
    hidden = (silu_gate * up).astype(jnp.bfloat16)
    across = (((1,), (1,)), ((), ()))
    d_hidden = lax.dot_general(rows_grad, w_down, across, preferred_element_type=jnp.float32)
    d_gate = (d_hidden * up * sig * (1.0 + gate * (1.0 - sig))).astype(jnp.bfloat16)
    d_up = (d_hidden * silu_gate).astype(jnp.bfloat16)
    grad_down = lax.dot_general(
        hidden, rows_grad, over_rows, preferred_element_type=jnp.float32
    ).astype(jnp.bfloat16)
    grad_gate = lax.dot_general(
        rows_input, d_gate, over_rows, preferred_element_type=jnp.float32
    ).astype(jnp.bfloat16)
    grad_up = lax.dot_general(
        rows_input, d_up, over_rows, preferred_element_type=jnp.float32
    ).astype(jnp.bfloat16)
    chunks = 2
    piece = capacity // chunks
    shape = (sp_devices, chunks, piece, d_gate.shape[1])
    gate_pieces = d_gate.reshape(shape)
    up_pieces = d_up.reshape(shape)
    shares = []
    for c in range(chunks):
        partial_input = lax.dot_general(
            gate_pieces[:, c].reshape(-1, shape[3]), w_gate, across,
            preferred_element_type=jnp.float32,
        ) + lax.dot_general(
            up_pieces[:, c].reshape(-1, shape[3]), w_up, across,
            preferred_element_type=jnp.float32,
        )
        shares.append(
            lax.psum_scatter(
                partial_input.astype(jnp.bfloat16), "tp", scatter_dimension=1, tiled=True
            )
        )
    shares[0], grad_down, grad_gate, grad_up = lax.optimization_barrier(
        (shares[0], grad_down, grad_gate, grad_up)
    )
    moe_grad = own_cotangent.astype(jnp.float32)
    pick_pieces = pick.reshape(experts, chunks, piece, tokens_here)
    for c in range(chunks):
        returned = to_owners(shares[c], sp_devices)
        moe_grad = moe_grad + lax.dot_general(
            pick_pieces[:, c].reshape(-1, tokens_here), returned, over_rows,
            preferred_element_type=jnp.float32,
        )
    stream_part = moe_grad.astype(jnp.bfloat16)
    stream_grad = lax.all_gather(stream_part, "tp", axis=1, tiled=True)
    own_projection = lax.dot_general(
        stream_grad, mixer_out, over_rows, preferred_element_type=jnp.float32
    ).astype(jnp.bfloat16)
    projections = to_owners(own_projection, sp_devices)
    grad_projection = jnp.sum(
        projections.astype(jnp.float32).reshape(sp_devices, -1, projections.shape[1]), axis=0
    )
    d_mixer = jnp.dot(stream_grad, out_proj, preferred_element_type=jnp.float32)
    grad_outer = d_mixer * conv_out
    d_conv = d_mixer * outer_gate.astype(jnp.float32)
    following = passed_along(d_conv[:2], "sp", -1)
    trailing = jnp.concatenate([d_conv, following], axis=0)
    d_mixed = (
        conv_taps[2] * trailing[:tokens_here]
        + conv_taps[1] * trailing[1 : tokens_here + 1]
        + conv_taps[0] * trailing[2:]
    )
    grad_inner = d_mixed * conv_input.astype(jnp.float32)
    grad_input = d_mixed * inner_gate.astype(jnp.float32)
    return (
        grad_gate[None],
        grad_up[None],
        grad_down[None],
        grad_projection,
        grad_outer,
        grad_inner,
        grad_input,
    )


def solution(mesh):
    placed = (
        P("sp", None),
        P("sp", None),
        P("sp", None),
        P("sp", None),
        P("sp", None, "tp"),
        P("sp", None, "tp"),
        P("sp", "tp", None),
        P("sp", "tp"),
        P("sp", "tp"),
        P("sp", "tp"),
        P(None, "tp"),
        P(None, "tp"),
    )
    return jax.shard_map(
        shards,
        mesh=mesh,
        in_specs=placed,
        out_specs=(
            P("sp", None, "tp"),
            P("sp", None, "tp"),
            P("sp", "tp", None),
            P("sp", "tp"),
            P("sp", "tp"),
            P("sp", "tp"),
            P("sp", "tp"),
        ),
        check_vma=False,
    )
```

time: 400 us -> 252 us (0.63)
  waiting for transfers between devices: 293 us -> 110 us
  blocking collectives: 0 us -> 62 us
  local copies, waits for them, and re-layouts: 23.9 us -> 1.3 us
    all_to_all x3, waiting for transfers between devices: 190 us -> 17.4 us  [to_owners(): lax.all_to_all(blocks, 'sp', split_axis=0, concat_axis=0, tiled=True)]
    all_to_all x0 -> x2, blocking collectives: none -> 62 us  [to_owners(): lax.all_to_all(blocks, 'sp', split_axis=0, concat_axis=0, tiled=True)]
    reduce_scatter x1 -> x0, waiting for transfers between devices: 47.8 us -> none  [shards(): lax.psum_scatter(lax.dot_general(stream_grad, mixer_out, over_rows, prefe...]
    all_gather x0 -> x2, waiting for transfers between devices: none -> 26.6 us  [the longest x1 26.6 us: shards(): rows_grad = lax.all_gather(got_grad, 'tp', axis=1, tiled=True)]
    gather x4 -> x0, local copies, waits for them, and re-layouts: 17.4 us -> none  [the longest x1 6.09 us: shards(): jnp.concatenate([stream, zero_row], axis=0)[slot_token]]
    dot_general x2 -> x9, matrix products: 4.64 us -> 11.1 us  [the longest x2 4.25 us: shards(): lax.dot_general(up_pieces[:, c].reshape(-1, shape[3]), w_up, across, pref...]
    all_gather x1, waiting for transfers between devices: 10.2 us -> 15 us  [shards(): stream_grad = lax.all_gather(stream_part, 'tp', axis=1, tiled=True)]
    ppermute x2, waiting for transfers between devices: 1.26 us -> 5.43 us  [passed_along(): return lax.ppermute(x, axis, pairs)]
  transfers between devices with their start and end apart: 8 -> 10, of which waited for: 7 -> 8; matrix products, arithmetic and copies ran while one was open for 9% -> 11% of each run, Pallas kernels for 0% -> 0%
where the time goes in v1:
time: 252 us; the launch traced here: 251 us
  waiting for transfers between devices  110 us (44%)
  blocking collectives  62 us (25%)
  matrix products  36.9 us (15%)
  starting transfers between devices  21.8 us (9%)
  between operations  14.1 us (6%)
  other arithmetic  5.08 us (2%)
    all_to_all x2, blocking collectives, to_owners(): lax.all_to_all(blocks, 'sp', split_axis=0, concat_axis=0, tiled=True)  62 us
    reduce_scatter x2, waiting for transfers between devices, shards(): lax.psum_scatter(partial_input.astype(jnp.bfloat16), 'tp', scatter_dimens...  45.6 us
    all_gather x1, waiting for transfers between devices, shards(): rows_grad = lax.all_gather(got_grad, 'tp', axis=1, tiled=True)  26.6 us
    all_to_all x3, waiting for transfers between devices, to_owners(): lax.all_to_all(blocks, 'sp', split_axis=0, concat_axis=0, tiled=True)  17.4 us
    all_to_all x3, starting transfers between devices, to_owners(): lax.all_to_all(blocks, 'sp', split_axis=0, concat_axis=0, tiled=True)  16.7 us
    all_gather x1, waiting for transfers between devices, shards(): stream_grad = lax.all_gather(stream_part, 'tp', axis=1, tiled=True)  15 us
    ppermute x2, waiting for transfers between devices, passed_along(): return lax.ppermute(x, axis, pairs)  5.43 us
  transfers between devices with their start and end apart: 10, of which 8 were waited for; matrix products, arithmetic and copies ran while one was open for 11% of the time, Pallas kernels for 0%

profile of v1, /device:TPU:0, one launch (start us, length us, event | category | flops | bytes accessed | tf_op | source)
XLA Modules:
  0.0 251.3 jit_solution(18357466165990084923)
XLA Ops:
  7.2 0.0 all-gather.6.cloned.1.call-start
  7.3 0.8 fusion.28
  8.0 0.1 convolution_select_fusion
  8.2 0.2 bitcast_compare_fusion
  8.4 1.4 convolution_convert_fusion.4
  9.9 33.1 %all_to_all.25 = bf16[8,128,512]{2,1,0:T(8,128)(2,1)} all-to-all(bf16[8,128,512]{2,1,0:T(8,128)(2,1)S(1)} %bitcast.79), channel_id=1, replica_groups=mesh['sp'=8,'tp'=4] {'sp'}, dimensions={0} | all-to-all | bytes 2097152 | tf_op jit(solution)/shard_map/all_to_all | solution.py:15
  43.0 0.0 all-gather.4.cloned.1.call-start
  43.0 0.2 select_reduce_fusion
  43.3 1.4 multiply_convert_fusion
  44.7 29.0 %all_to_all.26 = bf16[8,128,512]{2,1,0:T(8,128)(2,1)} all-to-all(bf16[8,128,512]{2,1,0:T(8,128)(2,1)S(1)} %bitcast.78), channel_id=1, replica_groups=mesh['sp'=8,'tp'=4] {'sp'}, dimensions={0} | all-to-all | bytes 2097152 | tf_op jit(solution)/shard_map/all_to_all | solution.py:15
  73.7 0.0 reduce-scatter.3.cloned.1.call-start
  73.8 3.5 %collective-permute-start = (f32[2,128]{1,0:T(2,128)S(1)}, f32[2,128]{1,0:T(2,128)S(1)}, u32[]{:S(2)}, u32[]{:S(2)}) collective-permute-start(f32[2,128]{1,0:T(2,128)S(1)} %slice.63), channel_id=1, source_target_pairs={{0,4},{4,8},{8,12},{12,16},{16,20},{20,24},{24,28},{1,5},{5,9},{9,... | collective-permute-start | bytes 3080 | tf_op jit(solution)/shard_map/ppermute | solution.py:10
  77.3 1.3 collective-permute-done
  78.5 0.7 fusion.25
  79.2 4.6 %fusion.5 = f32[1024,256]{1,0:T(8,128)} fusion(bf16[1024,2048]{1,0:T(8,128)(2,1)} %all-gather.6.cloned.1.call-done, bf16[1,2048,256]{2,1,0:T(8,128)(2,1)S(1)} %copy-done), kind=kOutput, calls=%fused_computation.16 | convolution fusion | flops 1073741824 | bytes 6291456 | tf_op jit(solution)/shard_map/dot_general | solution.py:77
  83.8 2.3 fusion.9
  86.1 26.6 %all-gather.4.cloned.1.call-done = bf16[1024,2048]{1,0:T(8,128)(2,1)} async-done(((bf16[1024,512]{1,0:T(8,128)(2,1)}), bf16[1024,2048]{1,0:T(8,128)(2,1)}) %all-gather.4.cloned.1.call-update) | async-done | bytes 4194320 | tf_op jit(solution)/shard_map/all_gather | solution.py:63
  112.7 4.6 %multiply_convert_fusion.2 = (bf16[1024,256]{1,0:T(8,128)(2,1)S(1)}, bf16[1024,256]{1,0:T(8,128)(2,1)S(1)}) fusion(f32[1024,256]{1,0:T(8,128)} %fusion.5, f32[1024,256]{1,0:T(8,128)} %fusion.9, bf16[1024,2048]{1,0:T(8,128)(2,1)} %all-gather.4.cloned.1.call-done, bf16[1,256,2048]{2,1,0:T(8,128)(2,1)} %param.18), kind=kOutput, calls=%fused_computation.27 | convolution fusion | flops 1077149696 | bytes 8388608 | tf_op jit(solution)/shard_map/dot_general | solution.py:83
  117.4 0.7 fusion.3
  118.1 2.1 add_convert_fusion.1
  120.3 0.2 reduce-scatter.5.cloned.1.call-start
  120.5 0.7 fusion.1
  121.3 2.1 add_convert_fusion
  123.4 4.9 %convolution_convert_fusion = bf16[2048,256]{1,0:T(8,128)(2,1)} fusion(bf16[1024,2048]{1,0:T(8,128)(2,1)} %all-gather.6.cloned.1.call-done, bf16[1024,256]{1,0:T(8,128)(2,1)} %copy-done.2), kind=kOutput, calls=%fused_computation.2 | convolution fusion | flops 1074266112 | bytes 5767168 | tf_op jit(solution)/shard_map/dot_general | solution.py:92
  128.3 2.4 convolution_convert_fusion.1
  130.7 0.6 copy-done.13
  131.3 0.3 copy-done.14
  131.6 2.3 convolution_convert_fusion.2
  134.0 17.6 %reduce-scatter.3.cloned.1.call-done = bf16[512,512]{1,0:T(8,128)(2,1)} async-done(((bf16[512,2048]{1,0:T(8,128)(2,1)}), bf16[512,512]{1,0:T(8,128)(2,1)}) %reduce-scatter.3.cloned.1.call-update) | async-done | bytes 524304 | tf_op jit(solution)/shard_map/reduce_scatter | solution.py:110
  151.6 5.6 %all-to-all-start.2 = ((bf16[8,64,512]{2,1,0:T(8,128)(2,1)}), bf16[8,64,512]{2,1,0:T(8,128)(2,1)S(1)}, u32[]{:S(2)}, u32[]{:S(2)}) async-start(bf16[8,64,512]{2,1,0:T(8,128)(2,1)} %bitcast.87), calls=%async_computation.3 | async-start | bytes 1048576 | tf_op jit(solution)/shard_map/all_to_all | solution.py:15
  157.3 27.9 %reduce-scatter.5.cloned.1.call-done = bf16[512,512]{1,0:T(8,128)(2,1)} async-done(((bf16[512,2048]{1,0:T(8,128)(2,1)}), bf16[512,512]{1,0:T(8,128)(2,1)}) %reduce-scatter.5.cloned.1.call-update) | async-done | bytes 524304 | tf_op jit(solution)/shard_map/reduce_scatter | solution.py:110
  185.2 5.5 %all-to-all-start.3 = ((bf16[8,64,512]{2,1,0:T(8,128)(2,1)}), bf16[8,64,512]{2,1,0:T(8,128)(2,1)S(1)}, u32[]{:S(2)}, u32[]{:S(2)}) async-start(bf16[8,64,512]{2,1,0:T(8,128)(2,1)} %bitcast.86), calls=%async_computation.5 | async-start | bytes 1048576 | tf_op jit(solution)/shard_map/all_to_all | solution.py:15
  190.7 0.0 all-gather.8.cloned.1.call-start
  190.8 0.2 broadcast_compare_fusion
  191.0 0.2 fusion.36
  191.2 1.3 convolution_add_fusion.1
  192.5 12.5 %all-to-all-done.3 = bf16[8,64,512]{2,1,0:T(8,128)(2,1)S(1)} async-done(((bf16[8,64,512]{2,1,0:T(8,128)(2,1)}), bf16[8,64,512]{2,1,0:T(8,128)(2,1)S(1)}, u32[]{:S(2)}, u32[]{:S(2)}) %all-to-all-start.3) | async-done | bytes 524320 | tf_op jit(solution)/shard_map/all_to_all | solution.py:15
  205.0 1.1 fusion
  206.1 15.0 %all-gather.8.cloned.1.call-done = bf16[256,2048]{1,0:T(8,128)(2,1)} async-done(((bf16[256,512]{1,0:T(8,128)(2,1)}), bf16[256,2048]{1,0:T(8,128)(2,1)}) %all-gather.8.cloned.1.call-update) | async-done | bytes 1048592 | tf_op jit(solution)/shard_map/all_gather | solution.py:126
  221.1 2.5 convolution_convert_fusion.3
  223.6 5.5 %all-to-all-start.4 = ((bf16[8,256,128]{2,1,0:T(8,128)(2,1)}), bf16[8,256,128]{2,1,0:T(8,128)(2,1)S(1)}, u32[]{:S(2)}, u32[]{:S(2)}) async-start(bf16[8,256,128]{2,1,0:T(8,128)(2,1)} %bitcast.30), calls=%async_computation.6 | async-start | bytes 1048576 | tf_op jit(solution)/shard_map/all_to_all | solution.py:15
  229.2 2.3 convert_multiply_fusion
  231.5 1.3 collective-permute-start.1
  232.8 4.2 %collective-permute-done.1 = f32[2,128]{1,0:T(2,128)S(1)} collective-permute-done((f32[2,128]{1,0:T(2,128)S(1)}, f32[2,128]{1,0:T(2,128)S(1)}, u32[]{:S(2)}, u32[]{:S(2)}) %collective-permute-start.1) | collective-permute-done | bytes 1056 | tf_op jit(solution)/shard_map/ppermute | solution.py:10
  236.9 1.5 convert_multiply_fusion.4
  238.5 0.7 convert_multiply_fusion.2
  239.1 4.9 %all-to-all-done.4 = bf16[8,256,128]{2,1,0:T(8,128)(2,1)S(1)} async-done(((bf16[8,256,128]{2,1,0:T(8,128)(2,1)}), bf16[8,256,128]{2,1,0:T(8,128)(2,1)S(1)}, u32[]{:S(2)}, u32[]{:S(2)}) %all-to-all-start.4) | async-done | bytes 524320 | tf_op jit(solution)/shard_map/all_to_all | solution.py:15
  244.0 0.7 convert_reduce_fusion
  (44 shorter events, 0.3 us)
Async XLA Ops:
  7.2 72.1 %copy-start = (bf16[1,2048,256]{2,1,0:T(8,128)(2,1)S(1)}, bf16[1,2048,256]{2,1,0:T(8,128)(2,1)}, u32[]{:S(2)}) copy-start(bf16[1,2048,256]{2,1,0:T(8,128)(2,1)} %param.16) | copy-start | bytes 3145732
  7.2 35.8 %copy-start.7 = (s32[256,2]{0,1:T(2,128)S(1)}, s32[256,2]{0,1:T(2,128)}, u32[]{:S(2)}) copy-start(s32[256,2]{0,1:T(2,128)} %param.14) | copy-start | bytes 6148
  7.2 35.8 %copy-start.8 = (f32[256,2]{0,1:T(2,128)S(1)}, f32[256,2]{0,1:T(2,128)}, u32[]{:S(2)}) copy-start(f32[256,2]{0,1:T(2,128)} %param.15) | copy-start | bytes 6148
  7.2 72.0 %all-gather.6.cloned.1.call-start = ((), (), s32[]{:S(2)}) async-start(), calls=%async_computation.8 | async-start | bytes 5242880 | tf_op jit(solution)/shard_map/all_gather | solution.py:60
  9.8 63.9 %copy-start.5 = (bf16[256,128]{1,0:T(8,128)(2,1)S(1)}, bf16[256,128]{1,0:T(8,128)(2,1)}, u32[]{:S(2)}) copy-start(bf16[256,128]{1,0:T(8,128)(2,1)} %param.21) | copy-start | bytes 196612
  9.8 63.9 %copy-start.6 = (bf16[256,128]{1,0:T(8,128)(2,1)S(1)}, bf16[256,128]{1,0:T(8,128)(2,1)}, u32[]{:S(2)}) copy-start(bf16[256,128]{1,0:T(8,128)(2,1)} %param.20) | copy-start | bytes 196612
  9.8 67.4 %copy-start.9 = (f32[3,128]{1,0:T(4,128)S(1)}, f32[3,128]{1,0:T(4,128)}, u32[]{:S(2)}) copy-start(f32[3,128]{1,0:T(4,128)} %param.22) | copy-start | bytes 4612
  9.8 68.7 %copy-start.4 = (bf16[256,128]{1,0:T(8,128)(2,1)S(1)}, bf16[256,128]{1,0:T(8,128)(2,1)}, u32[]{:S(2)}) copy-start(bf16[256,128]{1,0:T(8,128)(2,1)} %param.19) | copy-start | bytes 196612
  43.0 69.7 %all-gather.4.cloned.1.call-start = ((), (), s32[]{:S(2)}) async-start(), calls=%async_computation.7 | async-start | bytes 5242880 | tf_op jit(solution)/shard_map/all_gather | solution.py:63
  73.7 10.1 %copy-start.1 = (bf16[1,2048,256]{2,1,0:T(8,128)(2,1)S(1)}, bf16[1,2048,256]{2,1,0:T(8,128)(2,1)}, u32[]{:S(2)}) copy-start(bf16[1,2048,256]{2,1,0:T(8,128)(2,1)} %param.17) | copy-start | bytes 3145732
  73.7 78.0 %reduce-scatter.3.cloned.1.call-start = ((), (), s32[]{:S(2)}) async-start(), calls=%async_computation.9 | async-start | bytes 2621440 | tf_op jit(solution)/shard_map/reduce_scatter | solution.py:110
  73.8 4.7 %collective-permute-start = (f32[2,128]{1,0:T(2,128)S(1)}, f32[2,128]{1,0:T(2,128)S(1)}, u32[]{:S(2)}, u32[]{:S(2)}) collective-permute-start(f32[2,128]{1,0:T(2,128)S(1)} %slice.63), channel_id=1, source_target_pairs={{0,4},{4,8},{8,12},{12,16},{16,20},{20,24},{24,28},{1,5},{5,9},{9,... | collective-permute-start | bytes 3080 | tf_op jit(solution)/shard_map/ppermute | solution.py:10
  79.2 4.6 %copy-start.10 = (bf16[1024,2048]{1,0:T(8,128)(2,1)S(1)}, bf16[1024,2048]{1,0:T(8,128)(2,1)}, u32[]{:S(2)}) copy-start(bf16[1024,2048]{1,0:T(8,128)(2,1)} %all-gather.6.cloned.1.call-done) | copy-start | bytes 12582916
  117.3 0.8 copy-start.2
  120.3 64.9 %reduce-scatter.5.cloned.1.call-start = ((), (), s32[]{:S(2)}) async-start(), calls=%async_computation.10 | async-start | bytes 2621440 | tf_op jit(solution)/shard_map/reduce_scatter | solution.py:110
  123.4 4.9 %copy-start.11 = (bf16[1024,2048]{1,0:T(8,128)(2,1)S(1)}, bf16[1024,2048]{1,0:T(8,128)(2,1)}, u32[]{:S(2)}) copy-start(bf16[1024,2048]{1,0:T(8,128)(2,1)} %all-gather.6.cloned.1.call-done) | copy-start | bytes 12582916
  128.3 2.4 copy-start.12
  128.3 3.0 %copy-start.13 = (f32[1024,256]{1,0:T(8,128)S(1)}, f32[1024,256]{1,0:T(8,128)}, u32[]{:S(2)}) copy-start(f32[1024,256]{1,0:T(8,128)} %fusion.5) | copy-start | bytes 3145732
  128.3 3.3 %copy-start.14 = (f32[1024,256]{1,0:T(8,128)S(1)}, f32[1024,256]{1,0:T(8,128)}, u32[]{:S(2)}) copy-start(f32[1024,256]{1,0:T(8,128)} %fusion.9) | copy-start | bytes 3145732
  151.6 77.5 %copy-start.3 = (bf16[2048,128]{1,0:T(8,128)(2,1)S(1)}, bf16[2048,128]{1,0:T(8,128)(2,1)}, u32[]{:S(2)}) copy-start(bf16[2048,128]{1,0:T(8,128)(2,1)} %param.23) | copy-start | bytes 1572868
  151.6 33.6 %all-to-all-start.2 = ((bf16[8,64,512]{2,1,0:T(8,128)(2,1)}), bf16[8,64,512]{2,1,0:T(8,128)(2,1)S(1)}, u32[]{:S(2)}, u32[]{:S(2)}) async-start(bf16[8,64,512]{2,1,0:T(8,128)(2,1)} %bitcast.87), calls=%async_computation.3 | async-start | bytes 1048576 | tf_op jit(solution)/shard_map/all_to_all | solution.py:15
  185.2 19.8 %all-to-all-start.3 = ((bf16[8,64,512]{2,1,0:T(8,128)(2,1)}), bf16[8,64,512]{2,1,0:T(8,128)(2,1)S(1)}, u32[]{:S(2)}, u32[]{:S(2)}) async-start(bf16[8,64,512]{2,1,0:T(8,128)(2,1)} %bitcast.86), calls=%async_computation.5 | async-start | bytes 1048576 | tf_op jit(solution)/shard_map/all_to_all | solution.py:15
  190.7 30.4 %all-gather.8.cloned.1.call-start = ((), (), s32[]{:S(2)}) async-start(), calls=%async_computation.11 | async-start | bytes 1310720 | tf_op jit(solution)/shard_map/all_gather | solution.py:126
  223.6 20.4 %all-to-all-start.4 = ((bf16[8,256,128]{2,1,0:T(8,128)(2,1)}), bf16[8,256,128]{2,1,0:T(8,128)(2,1)S(1)}, u32[]{:S(2)}, u32[]{:S(2)}) async-start(bf16[8,256,128]{2,1,0:T(8,128)(2,1)} %bitcast.30), calls=%async_computation.6 | async-start | bytes 1048576 | tf_op jit(solution)/shard_map/all_to_all | solution.py:15
  231.5 5.5 %collective-permute-start.1 = (f32[2,128]{1,0:T(2,128)S(1)}, f32[2,128]{1,0:T(2,128)S(1)}, u32[]{:S(2)}, u32[]{:S(2)}) collective-permute-start(f32[2,128]{1,0:T(2,128)S(1)} %slice.72), channel_id=1, source_target_pairs={{4,0},{8,4},{12,8},{16,12},{20,16},{24,20},{28,24},{5,1},{9,5},{13... | collective-permute-start | bytes 3080 | tf_op jit(solution)/shard_map/ppermute | solution.py:10
Sparse Core Ops, SparseCore 0:
  43.1 33.4 all-gather.5
  78.2 34.4 all-gather.3
  120.4 31.1 reduce-scatter.2
  154.0 31.1 reduce-scatter.4
  206.3 14.8 all-gather.7

commit v2 on v1

--- a/solution.py
+++ b/solution.py
@@ -13,6 +13,40 @@
 def to_owners(x, devices):
     blocks = x.reshape(devices, -1, x.shape[1])
     return lax.all_to_all(blocks, "sp", split_axis=0, concat_axis=0, tiled=True).reshape(x.shape)
+
+
+def partial_rows(d_gate, d_up, w_gate, w_up):
+    across = (((1,), (1,)), ((), ()))
+    total = lax.dot_general(
+        d_gate, w_gate, across, preferred_element_type=jnp.float32
+    ) + lax.dot_general(d_up, w_up, across, preferred_element_type=jnp.float32)
+    return total.astype(jnp.bfloat16)
+
+
+def reduced_quarter(d_gate, d_up, w_gate, w_up):
+    devices = lax.axis_size("tp")
+    if devices != 4:
+        return lax.psum_scatter(
+            partial_rows(d_gate, d_up, w_gate, w_up), "tp", scatter_dimension=1, tiled=True
+        )
+    quarter = w_gate.shape[0] // devices
+    me = lax.axis_index("tp")
+
+    def rows_of(w, *flips):
+        return jnp.concatenate(
+            [lax.dynamic_slice_in_dim(w, (me ^ flip) * quarter, quarter, 0) for flip in flips]
+        )
+
+    def swapped(x, flip):
+        return lax.ppermute(x, "tp", [(i, i ^ flip) for i in range(devices)])
+
+    sent = partial_rows(d_gate, d_up, rows_of(w_gate, 1, 3), rows_of(w_up, 1, 3))
+    got = swapped(sent, 1)
+    kept = partial_rows(d_gate, d_up, rows_of(w_gate, 0, 2), rows_of(w_up, 0, 2))
+    far = kept[:, quarter:].astype(jnp.float32) + got[:, quarter:].astype(jnp.float32)
+    near = kept[:, :quarter].astype(jnp.float32) + got[:, :quarter].astype(jnp.float32)
+    other = swapped(far.astype(jnp.bfloat16), 2)
+    return (near + other.astype(jnp.float32)).astype(jnp.bfloat16)
 
 
 def shards(
@@ -99,16 +133,12 @@
     up_pieces = d_up.reshape(shape)
     shares = []
     for c in range(chunks):
-        partial_input = lax.dot_general(
-            gate_pieces[:, c].reshape(-1, shape[3]), w_gate, across,
-            preferred_element_type=jnp.float32,
-        ) + lax.dot_general(
-            up_pieces[:, c].reshape(-1, shape[3]), w_up, across,
-            preferred_element_type=jnp.float32,
-        )
         shares.append(
-            lax.psum_scatter(
-                partial_input.astype(jnp.bfloat16), "tp", scatter_dimension=1, tiled=True
+            reduced_quarter(
+                gate_pieces[:, c].reshape(-1, shape[3]),
+                up_pieces[:, c].reshape(-1, shape[3]),
+                w_gate,
+                w_up,
             )
         )
     shares[0], grad_down, grad_gate, grad_up = lax.optimization_barrier(

time: 252 us -> 230 us (0.913)
  waiting for transfers between devices: 110 us -> 85.3 us
  matrix products: 36.9 us -> 31.6 us
  other arithmetic: 5.08 us -> 9.56 us
  local copies, waits for them, and re-layouts: 1.3 us -> 4.05 us
    reduce_scatter x2 -> x0, waiting for transfers between devices: 45.6 us -> none  [shards(): lax.psum_scatter(partial_input.astype(jnp.bfloat16), 'tp', scatter_dimens...]
    ppermute x0 -> x4, waiting for transfers between devices: none -> 23.6 us  [swapped(): return lax.ppermute(x, 'tp', [(i, i ^ flip) for i in range(devices)])]
    convert_element_type x0 -> x4, other arithmetic: none -> 4.57 us  [the longest x2 3.15 us: reduced_quarter(): return (near + other.astype(jnp.float32)).astype(jnp.bfloat16)]
    dot_general x1, matrix products: 4.88 us -> 2.34 us  [shards(): lax.dot_general(rows_input, d_up, over_rows, preferred_element_type=jnp.f...]
    dot_general x4 -> x8, matrix products: 5.74 us -> 4.78 us  [the longest x4 2.9 us: partial_rows(): lax.dot_general(d_up, w_up, across, preferred_element_type=jnp.float32)]
  transfers between devices with their start and end apart: 10 -> 12, of which waited for: 8 -> 7; matrix products, arithmetic and copies ran while one was open for 11% -> 13% of each run, Pallas kernels for 0% -> 0%
where the time goes in v2:
time: 230 us
  waiting for transfers between devices  85.3 us (37%)
  blocking collectives  61.9 us (27%)
  matrix products  31.6 us (14%)
  starting transfers between devices  23 us (10%)
  between operations  14.1 us (6%)
  other arithmetic  9.56 us (4%)
  local copies, waits for them, and re-layouts  4.05 us (2%)
    all_to_all x2, blocking collectives, to_owners(): lax.all_to_all(blocks, 'sp', split_axis=0, concat_axis=0, tiled=True)  61.9 us
    all_gather x1, waiting for transfers between devices, shards(): rows_grad = lax.all_gather(got_grad, 'tp', axis=1, tiled=True)  24.7 us
    ppermute x4, waiting for transfers between devices, swapped(): return lax.ppermute(x, 'tp', [(i, i ^ flip) for i in range(devices)])  23.6 us
    all_to_all x3, waiting for transfers between devices, to_owners(): lax.all_to_all(blocks, 'sp', split_axis=0, concat_axis=0, tiled=True)  17.8 us
    all_to_all x3, starting transfers between devices, to_owners(): lax.all_to_all(blocks, 'sp', split_axis=0, concat_axis=0, tiled=True)  16.7 us
    all_gather x1, waiting for transfers between devices, shards(): stream_grad = lax.all_gather(stream_part, 'tp', axis=1, tiled=True)  15 us
    dot_general x1, matrix products, shards(): gate = jnp.dot(rows_input, w_gate, preferred_element_type=jnp.float32)  4.86 us
    dot_general x1, matrix products, shards(): lax.dot_general(rows_grad, w_down, across, preferred_element_type=jnp.flo...  4.61 us
  transfers between devices with their start and end apart: 12, of which 7 were waited for; matrix products, arithmetic and copies ran while one was open for 13% of the time, Pallas kernels for 0%

profile of v2, /device:TPU:0, one launch (start us, length us, event | category | flops | bytes accessed | tf_op | source)
XLA Modules:
  0.0 229.5 jit_solution(2613695500812486552)
XLA Ops:
  7.3 0.8 fusion.26
  8.4 0.5 convolution_convert_fusion.4
  8.9 32.9 %all_to_all.25 = bf16[8,128,512]{2,1,0:T(8,128)(2,1)} all-to-all(bf16[8,128,512]{2,1,0:T(8,128)(2,1)S(1)} %bitcast.91), channel_id=1, replica_groups=mesh['sp'=8,'tp'=4] {'sp'}, dimensions={0} | all-to-all | bytes 2097152 | tf_op jit(solution)/shard_map/all_to_all | solution.py:15
  42.2 1.4 multiply_convert_fusion
  43.6 29.0 %all_to_all.26 = bf16[8,128,512]{2,1,0:T(8,128)(2,1)} all-to-all(bf16[8,128,512]{2,1,0:T(8,128)(2,1)S(1)} %bitcast.90), channel_id=1, replica_groups=mesh['sp'=8,'tp'=4] {'sp'}, dimensions={0} | all-to-all | bytes 2097152 | tf_op jit(solution)/shard_map/all_to_all | solution.py:15
  72.7 3.3 %collective-permute-start = (f32[2,128]{1,0:T(2,128)S(1)}, f32[2,128]{1,0:T(2,128)S(1)}, u32[]{:S(2)}, u32[]{:S(2)}) collective-permute-start(f32[2,128]{1,0:T(2,128)S(1)} %slice.95), channel_id=1, source_target_pairs={{0,4},{4,8},{8,12},{12,16},{16,20},{20,24},{24,28},{1,5},{5,9},{9,... | collective-permute-start | bytes 3080 | tf_op jit(solution)/shard_map/ppermute | solution.py:10
  76.1 1.7 dynamic-slice_bitcast_fusion.5
  77.8 0.6 copy-done.14
  78.3 1.4 fusion.23
  79.8 4.9 %fusion.1 = f32[1024,256]{1,0:T(8,128)} fusion(bf16[1024,2048]{1,0:T(8,128)(2,1)} %all-gather.6.cloned.1.call-done, bf16[1,2048,256]{2,1,0:T(8,128)(2,1)} %param.16), kind=kOutput, calls=%fused_computation.14 | convolution fusion | flops 1073741824 | bytes 6291456 | tf_op jit(solution)/shard_map/dot_general | solution.py:111
  84.7 2.2 fusion.3
  86.9 24.7 %all-gather.4.cloned.1.call-done = bf16[1024,2048]{1,0:T(8,128)(2,1)} async-done(((bf16[1024,512]{1,0:T(8,128)(2,1)}), bf16[1024,2048]{1,0:T(8,128)(2,1)}) %all-gather.4.cloned.1.call-update) | async-done | bytes 4194320 | tf_op jit(solution)/shard_map/all_gather | solution.py:97
  111.6 4.6 %multiply_convert_fusion.2 = (bf16[1024,256]{1,0:T(8,128)(2,1)S(1)}, bf16[1024,256]{1,0:T(8,128)(2,1)S(1)}) fusion(f32[1024,256]{1,0:T(8,128)} %fusion.1, f32[1024,256]{1,0:T(8,128)} %fusion.3, bf16[1024,2048]{1,0:T(8,128)(2,1)} %all-gather.4.cloned.1.call-done, bf16[1,256,2048]{2,1,0:T(8,128)(2,1)} %param.18), kind=kOutput, calls=%fused_computation.27 | convolution fusion | flops 1077149696 | bytes 8388608 | tf_op jit(solution)/shard_map/dot_general | solution.py:117
  116.2 0.5 fusion.8
  116.7 0.5 fusion.9
  117.2 0.5 fusion.11
  117.6 0.5 fusion.10
  118.1 1.5 add_convert_fusion
  119.9 0.5 add_convert_fusion.2
  120.3 0.3 collective-permute-start.1
  120.7 0.5 add_convert_fusion.3
  121.2 0.5 add_convert_fusion.1
  121.6 1.2 copy-done.16
  122.9 2.3 %convolution_convert_fusion = bf16[2048,256]{1,0:T(8,128)(2,1)} fusion(bf16[1024,2048]{1,0:T(8,128)(2,1)S(1)} %copy-done.16, bf16[1024,256]{1,0:T(8,128)(2,1)S(1)} %get-tuple-element.27), kind=kOutput, calls=%fused_computation | convolution fusion | flops 1074266112 | bytes 5767168 | tf_op jit(solution)/shard_map/dot_general | solution.py:126
  125.2 2.3 %convolution_convert_fusion.1 = bf16[2048,256]{1,0:T(8,128)(2,1)} fusion(bf16[1024,2048]{1,0:T(8,128)(2,1)S(1)} %copy-done.16, bf16[1024,256]{1,0:T(8,128)(2,1)S(1)} %get-tuple-element.28), kind=kOutput, calls=%fused_computation.1 | convolution fusion | flops 1074266112 | bytes 5767168 | tf_op jit(solution)/shard_map/dot_general | solution.py:123
  127.8 0.4 collective-permute-start.2
  128.4 2.3 %convolution_convert_fusion.2 = bf16[256,2048]{1,0:T(8,128)(2,1)} fusion(bf16[1024,2048]{1,0:T(8,128)(2,1)S(1)} %copy-done.17, f32[1024,256]{1,0:T(8,128)S(1)} %copy-done.19, f32[1024,256]{1,0:T(8,128)S(1)} %copy-done.18), kind=kOutput, calls=%fused_computation.2 | convolution fusion | flops 1075838976 | bytes 7340032 | tf_op jit(solution)/shard_map/dot_general | solution.py:120
  130.7 11.2 %collective-permute-done.2 = bf16[512,512]{1,0:T(8,128)(2,1)S(1)} collective-permute-done((bf16[512,512]{1,0:T(8,128)(2,1)S(1)}, bf16[512,512]{1,0:T(8,128)(2,1)S(1)}, u32[]{:S(2)}, u32[]{:S(2)}) %collective-permute-start.2) | collective-permute-done | bytes 524320 | tf_op jit(solution)/shard_map/ppermute | solution.py:41
  141.9 1.1 add_convert_fusion.6
  143.0 5.5 %all-to-all-start.2 = ((bf16[8,64,512]{2,1,0:T(8,128)(2,1)}), bf16[8,64,512]{2,1,0:T(8,128)(2,1)S(1)}, u32[]{:S(2)}, u32[]{:S(2)}) async-start(bf16[8,64,512]{2,1,0:T(8,128)(2,1)} %bitcast.31), calls=%async_computation.2 | async-start | bytes 1048576 | tf_op jit(solution)/shard_map/all_to_all | solution.py:15
  148.5 1.2 add_convert_fusion.5
  149.7 0.6 collective-permute-start.4
  150.3 12.4 %collective-permute-done.4 = bf16[512,512]{1,0:T(8,128)(2,1)S(1)} collective-permute-done((bf16[512,512]{1,0:T(8,128)(2,1)S(1)}, bf16[512,512]{1,0:T(8,128)(2,1)S(1)}, u32[]{:S(2)}, u32[]{:S(2)}) %collective-permute-start.4) | collective-permute-done | bytes 524320 | tf_op jit(solution)/shard_map/ppermute | solution.py:41
  162.7 2.1 add_convert_fusion.4
  164.8 5.7 %all-to-all-start.3 = ((bf16[8,64,512]{2,1,0:T(8,128)(2,1)}), bf16[8,64,512]{2,1,0:T(8,128)(2,1)S(1)}, u32[]{:S(2)}, u32[]{:S(2)}) async-start(bf16[8,64,512]{2,1,0:T(8,128)(2,1)} %bitcast.36), calls=%async_computation.3 | async-start | bytes 1048576 | tf_op jit(solution)/shard_map/all_to_all | solution.py:15
  171.0 1.3 convolution_add_fusion.1
  172.3 10.9 %all-to-all-done.3 = bf16[8,64,512]{2,1,0:T(8,128)(2,1)S(1)} async-done(((bf16[8,64,512]{2,1,0:T(8,128)(2,1)}), bf16[8,64,512]{2,1,0:T(8,128)(2,1)S(1)}, u32[]{:S(2)}, u32[]{:S(2)}) %all-to-all-start.3) | async-done | bytes 524320 | tf_op jit(solution)/shard_map/all_to_all | solution.py:15
  183.2 1.0 fusion
  184.3 15.0 %all-gather.8.cloned.1.call-done = bf16[256,2048]{1,0:T(8,128)(2,1)} async-done(((bf16[256,512]{1,0:T(8,128)(2,1)}), bf16[256,2048]{1,0:T(8,128)(2,1)}) %all-gather.8.cloned.1.call-update) | async-done | bytes 1048592 | tf_op jit(solution)/shard_map/all_gather | solution.py:156
  199.2 2.6 %convolution_convert_fusion.3 = bf16[2048,128]{1,0:T(8,128)(2,1)} fusion(bf16[256,2048]{1,0:T(8,128)(2,1)} %all-gather.8.cloned.1.call-done, bf16[256,128]{1,0:T(8,128)(2,1)S(1)} %copy-done.6), kind=kOutput, calls=%fused_computation.3 | convolution fusion | flops 134479872 | bytes 1638400 | tf_op jit(solution)/shard_map/dot_general | solution.py:157
  201.8 5.5 %all-to-all-start.4 = ((bf16[8,256,128]{2,1,0:T(8,128)(2,1)}), bf16[8,256,128]{2,1,0:T(8,128)(2,1)S(1)}, u32[]{:S(2)}, u32[]{:S(2)}) async-start(bf16[8,256,128]{2,1,0:T(8,128)(2,1)} %bitcast.38), calls=%async_computation.4 | async-start | bytes 1048576 | tf_op jit(solution)/shard_map/all_to_all | solution.py:15
  207.4 1.1 convert_multiply_fusion
  208.5 1.3 collective-permute-start.5
  209.8 4.2 %collective-permute-done.5 = f32[2,128]{1,0:T(2,128)S(1)} collective-permute-done((f32[2,128]{1,0:T(2,128)S(1)}, f32[2,128]{1,0:T(2,128)S(1)}, u32[]{:S(2)}, u32[]{:S(2)}) %collective-permute-start.5) | collective-permute-done | bytes 1056 | tf_op jit(solution)/shard_map/ppermute | solution.py:10
  213.9 0.7 convert_multiply_fusion.4
  214.6 0.7 convert_multiply_fusion.2
  215.3 6.9 %all-to-all-done.4 = bf16[8,256,128]{2,1,0:T(8,128)(2,1)S(1)} async-done(((bf16[8,256,128]{2,1,0:T(8,128)(2,1)}), bf16[8,256,128]{2,1,0:T(8,128)(2,1)S(1)}, u32[]{:S(2)}, u32[]{:S(2)}) %all-to-all-start.4) | async-done | bytes 524320 | tf_op jit(solution)/shard_map/all_to_all | solution.py:15
  222.2 0.7 convert_reduce_fusion
  (65 shorter events, 2.0 us)
Async XLA Ops:
  7.2 1.2 copy-start
  7.2 72.6 %all-gather.6.cloned.1.call-start = ((), (), s32[]{:S(2)}) async-start(), calls=%async_computation.6 | async-start | bytes 5242880 | tf_op jit(solution)/shard_map/all_gather | solution.py:94
  8.4 33.5 %copy-start.9 = (s32[256,2]{0,1:T(2,128)S(1)}, s32[256,2]{0,1:T(2,128)}, u32[]{:S(2)}) copy-start(s32[256,2]{0,1:T(2,128)} %param.14) | copy-start | bytes 6148
  8.4 33.5 %copy-start.12 = (f32[256,2]{0,1:T(2,128)S(1)}, f32[256,2]{0,1:T(2,128)}, u32[]{:S(2)}) copy-start(f32[256,2]{0,1:T(2,128)} %param.15) | copy-start | bytes 6148
  41.9 69.7 %all-gather.4.cloned.1.call-start = ((), (), s32[]{:S(2)}) async-start(), calls=%async_computation.5 | async-start | bytes 5242880 | tf_op jit(solution)/shard_map/all_gather | solution.py:97
  42.2 30.5 %copy-start.5 = (bf16[256,128]{1,0:T(8,128)(2,1)S(1)}, bf16[256,128]{1,0:T(8,128)(2,1)}, u32[]{:S(2)}) copy-start(bf16[256,128]{1,0:T(8,128)(2,1)} %param.21) | copy-start | bytes 196612
  42.2 30.5 %copy-start.7 = (bf16[256,128]{1,0:T(8,128)(2,1)S(1)}, bf16[256,128]{1,0:T(8,128)(2,1)}, u32[]{:S(2)}) copy-start(bf16[256,128]{1,0:T(8,128)(2,1)} %param.20) | copy-start | bytes 196612
  43.6 32.4 %copy-start.13 = (f32[3,128]{1,0:T(4,128)S(1)}, f32[3,128]{1,0:T(4,128)}, u32[]{:S(2)}) copy-start(f32[3,128]{1,0:T(4,128)} %param.22) | copy-start | bytes 4612
  72.7 5.1 %collective-permute-start = (f32[2,128]{1,0:T(2,128)S(1)}, f32[2,128]{1,0:T(2,128)S(1)}, u32[]{:S(2)}, u32[]{:S(2)}) collective-permute-start(f32[2,128]{1,0:T(2,128)S(1)} %slice.95), channel_id=1, source_target_pairs={{0,4},{4,8},{8,12},{12,16},{16,20},{20,24},{24,28},{1,5},{5,9},{9,... | collective-permute-start | bytes 3080 | tf_op jit(solution)/shard_map/ppermute | solution.py:10
  76.0 2.3 copy-start.10
  76.1 2.3 copy-start.4
  77.8 0.6 copy-start.14
  79.8 4.9 %copy-start.2 = (bf16[1,2048,256]{2,1,0:T(8,128)(2,1)S(1)}, bf16[1,2048,256]{2,1,0:T(8,128)(2,1)}, u32[]{:S(2)}) copy-start(bf16[1,2048,256]{2,1,0:T(8,128)(2,1)} %param.17) | copy-start | bytes 3145732
  79.8 4.9 %copy-start.15 = (bf16[1024,2048]{1,0:T(8,128)(2,1)S(1)}, bf16[1024,2048]{1,0:T(8,128)(2,1)}, u32[]{:S(2)}) copy-start(bf16[1024,2048]{1,0:T(8,128)(2,1)} %all-gather.6.cloned.1.call-done) | copy-start | bytes 12582916
  119.6 28.9 %collective-permute-start.3 = (bf16[512,1024]{1,0:T(8,128)(2,1)}, bf16[512,1024]{1,0:T(8,128)(2,1)}, u32[]{:S(2)}, u32[]{:S(2)}) collective-permute-start(bf16[512,1024]{1,0:T(8,128)(2,1)} %add_convert_fusion), channel_id=1, source_target_pairs={{0,1},{1,0},{2,3},{3,2},{4,5},{5,4},{6,7},{7,6},{8,9},{9,8},{10,11... | collective-permute-start | bytes 3145736 | tf_op jit(solution)/shard_map/ppermute | solution.py:41
  120.3 7.2 %collective-permute-start.1 = (bf16[512,1024]{1,0:T(8,128)(2,1)S(1)}, bf16[512,1024]{1,0:T(8,128)(2,1)S(1)}, u32[]{:S(2)}, u32[]{:S(2)}) collective-permute-start(bf16[512,1024]{1,0:T(8,128)(2,1)S(1)} %add_convert_fusion.2), channel_id=1, source_target_pairs={{0,1},{1,0},{2,3},{3,2},{4,5},{5,4},{6,7},{7,6},{8,9},{9,8},{10,11... | collective-permute-start | bytes 3145736 | tf_op jit(solution)/shard_map/ppermute | solution.py:41
  120.7 2.2 copy-start.16
  125.2 3.0 %copy-start.17 = (bf16[1024,2048]{1,0:T(8,128)(2,1)S(1)}, bf16[1024,2048]{1,0:T(8,128)(2,1)}, u32[]{:S(2)}) copy-start(bf16[1024,2048]{1,0:T(8,128)(2,1)} %all-gather.4.cloned.1.call-done) | copy-start | bytes 12582916
  125.2 3.0 %copy-start.18 = (f32[1024,256]{1,0:T(8,128)S(1)}, f32[1024,256]{1,0:T(8,128)}, u32[]{:S(2)}) copy-start(f32[1024,256]{1,0:T(8,128)} %fusion.1) | copy-start | bytes 3145732
  125.2 3.2 %copy-start.19 = (f32[1024,256]{1,0:T(8,128)S(1)}, f32[1024,256]{1,0:T(8,128)}, u32[]{:S(2)}) copy-start(f32[1024,256]{1,0:T(8,128)} %fusion.3) | copy-start | bytes 3145732
  127.8 14.1 %collective-permute-start.2 = (bf16[512,512]{1,0:T(8,128)(2,1)S(1)}, bf16[512,512]{1,0:T(8,128)(2,1)S(1)}, u32[]{:S(2)}, u32[]{:S(2)}) collective-permute-start(bf16[512,512]{1,0:T(8,128)(2,1)S(1)} %add_convert_fusion.7), channel_id=1, source_target_pairs={{0,2},{1,3},{2,0},{3,1},{4,6},{5,7},{6,4},{7,5},{8,10},{9,11},{10,... | collective-permute-start | bytes 1572872 | tf_op jit(solution)/shard_map/ppermute | solution.py:41
  143.0 21.8 %all-to-all-start.2 = ((bf16[8,64,512]{2,1,0:T(8,128)(2,1)}), bf16[8,64,512]{2,1,0:T(8,128)(2,1)S(1)}, u32[]{:S(2)}, u32[]{:S(2)}) async-start(bf16[8,64,512]{2,1,0:T(8,128)(2,1)} %bitcast.31), calls=%async_computation.2 | async-start | bytes 1048576 | tf_op jit(solution)/shard_map/all_to_all | solution.py:15
  149.7 13.0 %collective-permute-start.4 = (bf16[512,512]{1,0:T(8,128)(2,1)S(1)}, bf16[512,512]{1,0:T(8,128)(2,1)S(1)}, u32[]{:S(2)}, u32[]{:S(2)}) collective-permute-start(bf16[512,512]{1,0:T(8,128)(2,1)S(1)} %add_convert_fusion.5), channel_id=1, source_target_pairs={{0,2},{1,3},{2,0},{3,1},{4,6},{5,7},{6,4},{7,5},{8,10},{9,11},{10,... | collective-permute-start | bytes 1572872 | tf_op jit(solution)/shard_map/ppermute | solution.py:41
  164.8 18.4 %all-to-all-start.3 = ((bf16[8,64,512]{2,1,0:T(8,128)(2,1)}), bf16[8,64,512]{2,1,0:T(8,128)(2,1)S(1)}, u32[]{:S(2)}, u32[]{:S(2)}) async-start(bf16[8,64,512]{2,1,0:T(8,128)(2,1)} %bitcast.36), calls=%async_computation.3 | async-start | bytes 1048576 | tf_op jit(solution)/shard_map/all_to_all | solution.py:15
  170.5 28.7 %copy-start.6 = (bf16[256,128]{1,0:T(8,128)(2,1)S(1)}, bf16[256,128]{1,0:T(8,128)(2,1)}, u32[]{:S(2)}) copy-start(bf16[256,128]{1,0:T(8,128)(2,1)} %get-tuple-element.21) | copy-start | bytes 196612
  170.5 28.7 %all-gather.8.cloned.1.call-start = ((), (), s32[]{:S(2)}) async-start(), calls=%async_computation.7 | async-start | bytes 1310720 | tf_op jit(solution)/shard_map/all_gather | solution.py:156
  183.2 24.2 %copy-start.3 = (bf16[2048,128]{1,0:T(8,128)(2,1)S(1)}, bf16[2048,128]{1,0:T(8,128)(2,1)}, u32[]{:S(2)}) copy-start(bf16[2048,128]{1,0:T(8,128)(2,1)} %param.23) | copy-start | bytes 1572868
  184.2 29.7 %copy-start.8 = (bf16[256,128]{1,0:T(8,128)(2,1)S(1)}, bf16[256,128]{1,0:T(8,128)(2,1)}, u32[]{:S(2)}) copy-start(bf16[256,128]{1,0:T(8,128)(2,1)} %param.20) | copy-start | bytes 196612
  184.3 29.7 %copy-start.11 = (f32[128]{0:T(128)S(1)}, f32[128]{0:T(128)}, u32[]{:S(2)}) copy-start(f32[128]{0:T(128)} %copy-done.10) | copy-start | bytes 1540
  199.2 8.1 %copy-start.1 = (bf16[256,2048]{1,0:T(8,128)(2,1)S(1)}, bf16[256,2048]{1,0:T(8,128)(2,1)}, u32[]{:S(2)}) copy-start(bf16[256,2048]{1,0:T(8,128)(2,1)} %all-gather.8.cloned.1.call-done) | copy-start | bytes 3145732
  201.8 20.4 %all-to-all-start.4 = ((bf16[8,256,128]{2,1,0:T(8,128)(2,1)}), bf16[8,256,128]{2,1,0:T(8,128)(2,1)S(1)}, u32[]{:S(2)}, u32[]{:S(2)}) async-start(bf16[8,256,128]{2,1,0:T(8,128)(2,1)} %bitcast.38), calls=%async_computation.4 | async-start | bytes 1048576 | tf_op jit(solution)/shard_map/all_to_all | solution.py:15
  208.5 5.5 %collective-permute-start.5 = (f32[2,128]{1,0:T(2,128)S(1)}, f32[2,128]{1,0:T(2,128)S(1)}, u32[]{:S(2)}, u32[]{:S(2)}) collective-permute-start(f32[2,128]{1,0:T(2,128)S(1)} %slice.112), channel_id=1, source_target_pairs={{4,0},{8,4},{12,8},{16,12},{20,16},{24,20},{28,24},{5,1},{9,5},{13... | collective-permute-start | bytes 3080 | tf_op jit(solution)/shard_map/ppermute | solution.py:10
Sparse Core Ops, SparseCore 0:
  42.0 33.4 all-gather.5
  77.1 34.4 all-gather.3
  184.4 14.8 all-gather.7

commit v3 on v2

--- a/solution.py
+++ b/solution.py
@@ -82,19 +82,26 @@
         hit.astype(jnp.bfloat16), below, over_rows, preferred_element_type=jnp.float32
     )
     rank = jnp.where(hit.T, rank, -1.0)
-    in_slot = rank[:, None, :] == jnp.arange(capacity, dtype=jnp.float32)[None, :, None]
-    slot_weight = jnp.sum(jnp.where(in_slot, token_weight.T[:, None, :], 0.0), axis=2)
-    pick = in_slot.astype(jnp.bfloat16).reshape(experts * capacity, tokens_here)
-    send_input = jnp.dot(pick, own_stream, preferred_element_type=jnp.float32).astype(jnp.bfloat16)
-    send_grad = (
-        slot_weight.reshape(-1, 1)
-        * jnp.dot(pick, own_cotangent, preferred_element_type=jnp.float32)
-    ).astype(jnp.bfloat16)
-    got_input = to_owners(send_input, sp_devices)
-    rows_input = lax.all_gather(got_input, "tp", axis=1, tiled=True)
-    send_grad, got_input = lax.optimization_barrier((send_grad, got_input))
-    got_grad = to_owners(send_grad, sp_devices)
-    rows_grad = lax.all_gather(got_grad, "tp", axis=1, tiled=True)
+    chunks = 2
+    piece = capacity // chunks
+    picks, inputs, grads = [], [], []
+    last = None
+    for c in range(chunks):
+        slots = jnp.arange(c * piece, (c + 1) * piece, dtype=jnp.int32).astype(jnp.float32)
+        in_slot = rank[:, None, :] == slots[None, :, None]
+        slot_weight = jnp.sum(jnp.where(in_slot, token_weight.T[:, None, :], 0.0), axis=2)
+        pick = in_slot.astype(jnp.bfloat16).reshape(experts * piece, tokens_here)
+        send_input = jnp.dot(pick, own_stream, preferred_element_type=jnp.float32)
+        send_grad = slot_weight.reshape(-1, 1) * jnp.dot(
+            pick, own_cotangent, preferred_element_type=jnp.float32
+        )
+        picks.append(pick)
+        for rows, send in ((inputs, send_input), (grads, send_grad)):
+            send = send.astype(jnp.bfloat16)
+            if last is not None:
+                send, last = lax.optimization_barrier((send, last))
+            last = to_owners(send, sp_devices)
+            rows.append(lax.all_gather(last, "tp", axis=1, tiled=True))
     mixed = inner_gate.astype(jnp.float32) * conv_input.astype(jnp.float32)
     previous = passed_along(mixed[tokens_here - 2 :], "sp", 1)
     extended = jnp.concatenate([previous, mixed], axis=0)
@@ -104,52 +111,43 @@
         + conv_taps[2] * extended[2:]
     )
     mixer_out = (outer_gate.astype(jnp.float32) * conv_out).astype(jnp.bfloat16)
-    conv_out, mixer_out, rows_grad = lax.optimization_barrier((conv_out, mixer_out, rows_grad))
+    conv_out, mixer_out, grads[0] = lax.optimization_barrier((conv_out, mixer_out, grads[0]))
     w_gate = gate_proj[0]
     w_up = up_proj[0]
     w_down = down_proj[0]
-    gate = jnp.dot(rows_input, w_gate, preferred_element_type=jnp.float32)
-    up = jnp.dot(rows_input, w_up, preferred_element_type=jnp.float32)
-    sig = jax.nn.sigmoid(gate)
-    silu_gate = gate * sig
-    hidden = (silu_gate * up).astype(jnp.bfloat16)
     across = (((1,), (1,)), ((), ()))
-    d_hidden = lax.dot_general(rows_grad, w_down, across, preferred_element_type=jnp.float32)
-    d_gate = (d_hidden * up * sig * (1.0 + gate * (1.0 - sig))).astype(jnp.bfloat16)
-    d_up = (d_hidden * silu_gate).astype(jnp.bfloat16)
-    grad_down = lax.dot_general(
-        hidden, rows_grad, over_rows, preferred_element_type=jnp.float32
-    ).astype(jnp.bfloat16)
-    grad_gate = lax.dot_general(
-        rows_input, d_gate, over_rows, preferred_element_type=jnp.float32
-    ).astype(jnp.bfloat16)
-    grad_up = lax.dot_general(
-        rows_input, d_up, over_rows, preferred_element_type=jnp.float32
-    ).astype(jnp.bfloat16)
-    chunks = 2
-    piece = capacity // chunks
-    shape = (sp_devices, chunks, piece, d_gate.shape[1])
-    gate_pieces = d_gate.reshape(shape)
-    up_pieces = d_up.reshape(shape)
     shares = []
-    for c in range(chunks):
-        shares.append(
-            reduced_quarter(
-                gate_pieces[:, c].reshape(-1, shape[3]),
-                up_pieces[:, c].reshape(-1, shape[3]),
-                w_gate,
-                w_up,
-            )
-        )
-    shares[0], grad_down, grad_gate, grad_up = lax.optimization_barrier(
-        (shares[0], grad_down, grad_gate, grad_up)
+    grad_down = grad_gate = grad_up = 0.0
+    for rows_input, rows_grad in zip(inputs, grads):
+        gate = jnp.dot(rows_input, w_gate, preferred_element_type=jnp.float32)
+        up = jnp.dot(rows_input, w_up, preferred_element_type=jnp.float32)
+        sig = jax.nn.sigmoid(gate)
+        silu_gate = gate * sig
+        hidden = (silu_gate * up).astype(jnp.bfloat16)
+        d_hidden = lax.dot_general(rows_grad, w_down, across, preferred_element_type=jnp.float32)
+        d_gate = (d_hidden * up * sig * (1.0 + gate * (1.0 - sig))).astype(jnp.bfloat16)
+        d_up = (d_hidden * silu_gate).astype(jnp.bfloat16)
+        shares.append(reduced_quarter(d_gate, d_up, w_gate, w_up))
+        grad_down += lax.dot_general(
+            hidden, rows_grad, over_rows, preferred_element_type=jnp.float32
+        )
+        grad_gate += lax.dot_general(
+            rows_input, d_gate, over_rows, preferred_element_type=jnp.float32
+        )
+        grad_up += lax.dot_general(
+            rows_input, d_up, over_rows, preferred_element_type=jnp.float32
+        )
+    grad_down = grad_down.astype(jnp.bfloat16)
+    grad_gate = grad_gate.astype(jnp.bfloat16)
+    grad_up = grad_up.astype(jnp.bfloat16)
+    shares[-1], grad_down, grad_gate, grad_up = lax.optimization_barrier(
+        (shares[-1], grad_down, grad_gate, grad_up)
     )
     moe_grad = own_cotangent.astype(jnp.float32)
-    pick_pieces = pick.reshape(experts, chunks, piece, tokens_here)
     for c in range(chunks):
         returned = to_owners(shares[c], sp_devices)
         moe_grad = moe_grad + lax.dot_general(
-            pick_pieces[:, c].reshape(-1, tokens_here), returned, over_rows,
+            picks[c], returned, over_rows,
             preferred_element_type=jnp.float32,
         )
     stream_part = moe_grad.astype(jnp.bfloat16)

time: 230 us -> 240 us (1.043)
  matrix products: 31.6 us -> 46.6 us
  waiting for transfers between devices: 85.3 us -> 78.5 us
  blocking collectives: 61.9 us -> 57.1 us
  starting transfers between devices: 23 us -> 27.3 us
  local copies, waits for them, and re-layouts: 4.05 us -> 6.79 us
    all_gather x2 -> x4, waiting for transfers between devices: 24.7 us -> 12.3 us  [shards(): rows.append(lax.all_gather(last, 'tp', axis=1, tiled=True))]
    all_to_all x3 -> x4, waiting for transfers between devices: 17.8 us -> 24.6 us  [to_owners(): lax.all_to_all(blocks, 'sp', split_axis=0, concat_axis=0, tiled=True)]
    all_to_all x2 -> x3, blocking collectives: 61.9 us -> 57.1 us  [to_owners(): lax.all_to_all(blocks, 'sp', split_axis=0, concat_axis=0, tiled=True)]
    all_to_all x3 -> x4, starting transfers between devices: 16.7 us -> 20.5 us  [to_owners(): lax.all_to_all(blocks, 'sp', split_axis=0, concat_axis=0, tiled=True)]
    dot_general x1 -> x2, matrix products: 2.25 us -> 5.03 us  [shards(): up = jnp.dot(rows_input, w_up, preferred_element_type=jnp.float32)]
    dot_general x1 -> x2, matrix products: 4.86 us -> 6.44 us  [shards(): gate = jnp.dot(rows_input, w_gate, preferred_element_type=jnp.float32)]
    dot_general x1 -> x2, matrix products: 4.61 us -> 6.06 us  [shards(): lax.dot_general(rows_grad, w_down, across, preferred_element_type=jnp.flo...]
  transfers between devices with their start and end apart: 12 -> 15, of which waited for: 7 -> 8; matrix products, arithmetic and copies ran while one was open for 13% -> 21% of each run, Pallas kernels for 0% -> 0%
where the time goes in v3:
time: 240 us; the launch traced here: 239 us
  waiting for transfers between devices  78.5 us (33%)
  blocking collectives  57.1 us (24%)
  matrix products  46.6 us (19%)
  starting transfers between devices  27.3 us (11%)
  between operations  14.4 us (6%)
  other arithmetic  8.68 us (4%)
  local copies, waits for them, and re-layouts  6.79 us (3%)
    all_to_all x3, blocking collectives, to_owners(): lax.all_to_all(blocks, 'sp', split_axis=0, concat_axis=0, tiled=True)  57.1 us
    all_to_all x4, waiting for transfers between devices, to_owners(): lax.all_to_all(blocks, 'sp', split_axis=0, concat_axis=0, tiled=True)  24.6 us
    ppermute x4, waiting for transfers between devices, swapped(): return lax.ppermute(x, 'tp', [(i, i ^ flip) for i in range(devices)])  22.3 us
    all_to_all x4, starting transfers between devices, to_owners(): lax.all_to_all(blocks, 'sp', split_axis=0, concat_axis=0, tiled=True)  20.5 us
    all_gather x1, waiting for transfers between devices, shards(): stream_grad = lax.all_gather(stream_part, 'tp', axis=1, tiled=True)  15 us
    all_gather x4, waiting for transfers between devices, shards(): rows.append(lax.all_gather(last, 'tp', axis=1, tiled=True))  12.3 us
    dot_general x2, matrix products, shards(): gate = jnp.dot(rows_input, w_gate, preferred_element_type=jnp.float32)  6.44 us
    dot_general x2, matrix products, shards(): lax.dot_general(rows_grad, w_down, across, preferred_element_type=jnp.flo...  6.06 us
  transfers between devices with their start and end apart: 15, of which 8 were waited for; matrix products, arithmetic and copies ran while one was open for 21% of the time, Pallas kernels for 0%

profile of v3, /device:TPU:0, one launch (start us, length us, event | category | flops | bytes accessed | tf_op | source)
XLA Modules:
  0.0 239.4 jit_solution(460060010115240534)
XLA Ops:
  7.3 0.8 fusion.52
  8.9 21.7 %all_to_all.35 = bf16[8,64,512]{2,1,0:T(8,128)(2,1)} all-to-all(bf16[8,64,512]{2,1,0:T(8,128)(2,1)S(1)} %bitcast.111), channel_id=1, replica_groups=mesh['sp'=8,'tp'=4] {'sp'}, dimensions={0} | all-to-all | bytes 1048576 | tf_op jit(solution)/shard_map/all_to_all | solution.py:15
  31.1 1.3 fusion.4
  32.4 17.6 %all_to_all.36 = bf16[8,64,512]{2,1,0:T(8,128)(2,1)} all-to-all(bf16[8,64,512]{2,1,0:T(8,128)(2,1)S(1)} %bitcast.110), channel_id=1, replica_groups=mesh['sp'=8,'tp'=4] {'sp'}, dimensions={0} | all-to-all | bytes 1048576 | tf_op jit(solution)/shard_map/all_to_all | solution.py:15
  50.5 17.7 %all_to_all.37 = bf16[8,64,512]{2,1,0:T(8,128)(2,1)} all-to-all(bf16[8,64,512]{2,1,0:T(8,128)(2,1)S(1)} %bitcast.112), channel_id=1, replica_groups=mesh['sp'=8,'tp'=4] {'sp'}, dimensions={0} | all-to-all | bytes 1048576 | tf_op jit(solution)/shard_map/all_to_all | solution.py:15
  68.3 2.1 fusion.3
  70.4 3.6 %all-to-all-start.3 = ((bf16[8,64,512]{2,1,0:T(8,128)(2,1)}), bf16[8,64,512]{2,1,0:T(8,128)(2,1)S(1)}, u32[]{:S(2)}, u32[]{:S(2)}) async-start(bf16[8,64,512]{2,1,0:T(8,128)(2,1)} %bitcast.9), calls=%async_computation.3 | async-start | bytes 1048576 | tf_op jit(solution)/shard_map/all_to_all | solution.py:15
  74.1 4.1 %collective-permute-start.2 = (f32[2,128]{1,0:T(2,128)S(1)}, f32[2,128]{1,0:T(2,128)S(1)}, u32[]{:S(2)}, u32[]{:S(2)}) collective-permute-start(f32[2,128]{1,0:T(2,128)S(1)} %slice.75), channel_id=1, source_target_pairs={{0,4},{4,8},{8,12},{12,16},{16,20},{20,24},{24,28},{1,5},{5,9},{9,... | collective-permute-start | bytes 3080 | tf_op jit(solution)/shard_map/ppermute | solution.py:10
  78.2 2.6 %dynamic-slice_bitcast_fusion.5 = (bf16[512,256]{1,0:T(8,128)(2,1)}, bf16[512,256]{1,0:T(8,128)(2,1)}, bf16[512,256]{1,0:T(8,128)(2,1)}, bf16[512,256]{1,0:T(8,1...) fusion(bf16[1,2048,256]{2,1,0:T(8,128)(2,1)} %param.17, ...), kind=kLoop, calls=%fused_computation.72 | loop fusion | bytes 4194320 | tf_op jit(solution)/shard_map/dynamic_slice | solution.py:37
  80.8 0.7 fusion.47
  81.5 6.6 %all-to-all-done.3 = bf16[8,64,512]{2,1,0:T(8,128)(2,1)S(1)} async-done(((bf16[8,64,512]{2,1,0:T(8,128)(2,1)}), bf16[8,64,512]{2,1,0:T(8,128)(2,1)S(1)}, u32[]{:S(2)}, u32[]{:S(2)}) %all-to-all-start.3) | async-done | bytes 524320 | tf_op jit(solution)/shard_map/all_to_all | solution.py:15
  88.1 0.8 copy-done.25
  89.0 3.5 %fusion.12 = f32[512,256]{1,0:T(8,128)} fusion(bf16[512,2048]{1,0:T(8,128)(2,1)} %all-gather.10.cloned.1.call-done, bf16[1,2048,256]{2,1,0:T(8,128)(2,1)} %param.17), kind=kOutput, calls=%fused_computation.27 | convolution fusion | flops 536870912 | bytes 3670016 | tf_op jit(solution)/shard_map/dot_general | solution.py:123
  92.5 2.7 %fusion.8 = f32[512,256]{1,0:T(8,128)} fusion(bf16[512,2048]{1,0:T(8,128)(2,1)S(1)} %copy-done.1, bf16[1,2048,256]{2,1,0:T(8,128)(2,1)} %param.16), kind=kOutput, calls=%fused_computation.23 | convolution fusion | flops 536870912 | bytes 3670016 | tf_op jit(solution)/shard_map/dot_general | solution.py:122
  95.2 3.0 %multiply_convert_fusion = (bf16[512,256]{1,0:T(8,128)(2,1)S(1)}, bf16[512,256]{1,0:T(8,128)(2,1)S(1)}) fusion(f32[512,256]{1,0:T(8,128)} %fusion.8, f32[512,256]{1,0:T(8,128)} %fusion.12, bf16[512,2048]{1,0:T(8,128)(2,1)} %all-gather.12.cloned.1.call-done, bf16[1,256,2048]{2,1,0:T(8,128)(2,1)} %param.18), kind=kOutput, calls=%fused_computation.52 | convolution fusion | flops 538574848 | bytes 4718592 | tf_op jit(solution)/shard_map/dot_general | solution.py:127
  99.3 1.5 add_convert_fusion
  100.8 1.9 fusion.28
  102.7 2.1 fusion.70
  104.7 2.1 fusion.69
  107.0 0.8 fusion.30
  107.9 3.7 %fusion.10 = f32[512,256]{1,0:T(8,128)} fusion(bf16[512,2048]{1,0:T(8,128)(2,1)} %all-gather.8.cloned.1.call-done, bf16[1,2048,256]{2,1,0:T(8,128)(2,1)} %param.16), kind=kOutput, calls=%fused_computation.25 | convolution fusion | flops 536870912 | bytes 3670016 | tf_op jit(solution)/shard_map/dot_general | solution.py:122
  111.6 1.5 fusion.14
  113.1 12.3 %all-gather.6.cloned.1.call-done = bf16[512,2048]{1,0:T(8,128)(2,1)} async-done(((bf16[512,512]{1,0:T(8,128)(2,1)}), bf16[512,2048]{1,0:T(8,128)(2,1)}) %all-gather.6.cloned.1.call-update) | async-done | bytes 2097168 | tf_op jit(solution)/shard_map/all_gather | solution.py:104
  125.4 3.0 %multiply_convert_fusion.4 = (bf16[512,256]{1,0:T(8,128)(2,1)S(1)}, bf16[512,256]{1,0:T(8,128)(2,1)S(1)}) fusion(f32[512,256]{1,0:T(8,128)} %fusion.10, f32[512,256]{1,0:T(8,128)} %fusion.14, bf16[512,2048]{1,0:T(8,128)(2,1)} %all-gather.6.cloned.1.call-done, bf16[1,256,2048]{2,1,0:T(8,128)(2,1)} %param.18), kind=kOutput, calls=%fused_computation.58 | convolution fusion | flops 538574848 | bytes 4718592 | tf_op jit(solution)/shard_map/dot_general | solution.py:127
  130.6 1.5 add_convert_fusion.1
  133.7 0.7 copy-done.3
  134.5 1.7 fusion.2
  136.9 1.7 fusion.1
  138.6 2.0 fusion
  140.6 10.0 %collective-permute-done.1 = bf16[512,512]{1,0:T(8,128)(2,1)S(1)} collective-permute-done((bf16[512,512]{1,0:T(8,128)(2,1)S(1)}, bf16[512,512]{1,0:T(8,128)(2,1)S(1)}, u32[]{:S(2)}, u32[]{:S(2)}) %collective-permute-start.1) | collective-permute-done | bytes 524320 | tf_op jit(solution)/shard_map/ppermute | solution.py:41
  150.6 1.1 add_convert_fusion.6
  151.7 5.5 %all-to-all-start.5 = ((bf16[8,64,512]{2,1,0:T(8,128)(2,1)}), bf16[8,64,512]{2,1,0:T(8,128)(2,1)S(1)}, u32[]{:S(2)}, u32[]{:S(2)}) async-start(bf16[8,64,512]{2,1,0:T(8,128)(2,1)} %bitcast.30), calls=%async_computation.5 | async-start | bytes 1048576 | tf_op jit(solution)/shard_map/all_to_all | solution.py:15
  157.2 1.2 add_convert_fusion.5
  159.1 12.4 %collective-permute-done.4 = bf16[512,512]{1,0:T(8,128)(2,1)S(1)} collective-permute-done((bf16[512,512]{1,0:T(8,128)(2,1)S(1)}, bf16[512,512]{1,0:T(8,128)(2,1)S(1)}, u32[]{:S(2)}, u32[]{:S(2)}) %collective-permute-start.4) | collective-permute-done | bytes 524320 | tf_op jit(solution)/shard_map/ppermute | solution.py:41
  171.5 2.1 add_convert_fusion.4
  173.5 5.7 %all-to-all-start.4 = ((bf16[8,64,512]{2,1,0:T(8,128)(2,1)}), bf16[8,64,512]{2,1,0:T(8,128)(2,1)S(1)}, u32[]{:S(2)}, u32[]{:S(2)}) async-start(bf16[8,64,512]{2,1,0:T(8,128)(2,1)} %bitcast.28), calls=%async_computation.4 | async-start | bytes 1048576 | tf_op jit(solution)/shard_map/all_to_all | solution.py:15
  179.8 12.1 %all-to-all-done.4 = bf16[8,64,512]{2,1,0:T(8,128)(2,1)S(1)} async-done(((bf16[8,64,512]{2,1,0:T(8,128)(2,1)}), bf16[8,64,512]{2,1,0:T(8,128)(2,1)S(1)}, u32[]{:S(2)}, u32[]{:S(2)}) %all-to-all-start.4) | async-done | bytes 524320 | tf_op jit(solution)/shard_map/all_to_all | solution.py:15
  191.9 2.1 fusion.7
  194.0 15.0 %all-gather.14.cloned.1.call-done = bf16[256,2048]{1,0:T(8,128)(2,1)} async-done(((bf16[256,512]{1,0:T(8,128)(2,1)}), bf16[256,2048]{1,0:T(8,128)(2,1)}) %all-gather.14.cloned.1.call-update) | async-done | bytes 1048592 | tf_op jit(solution)/shard_map/all_gather | solution.py:154
  209.0 2.6 %convolution_convert_fusion = bf16[2048,128]{1,0:T(8,128)(2,1)} fusion(bf16[256,2048]{1,0:T(8,128)(2,1)} %all-gather.14.cloned.1.call-done, bf16[256,128]{1,0:T(8,128)(2,1)S(1)} %copy-done.36), kind=kOutput, calls=%fused_computation.6 | convolution fusion | flops 134479872 | bytes 1638400 | tf_op jit(solution)/shard_map/dot_general | solution.py:155
  211.6 5.6 %all-to-all-start.6 = ((bf16[8,256,128]{2,1,0:T(8,128)(2,1)}), bf16[8,256,128]{2,1,0:T(8,128)(2,1)S(1)}, u32[]{:S(2)}, u32[]{:S(2)}) async-start(bf16[8,256,128]{2,1,0:T(8,128)(2,1)} %bitcast.32), calls=%async_computation.6 | async-start | bytes 1048576 | tf_op jit(solution)/shard_map/all_to_all | solution.py:15
  217.3 2.1 convert_multiply_fusion
  219.4 1.3 collective-permute-start.5
  220.7 4.2 %collective-permute-done.5 = f32[2,128]{1,0:T(2,128)S(1)} collective-permute-done((f32[2,128]{1,0:T(2,128)S(1)}, f32[2,128]{1,0:T(2,128)S(1)}, u32[]{:S(2)}, u32[]{:S(2)}) %collective-permute-start.5) | collective-permute-done | bytes 1056 | tf_op jit(solution)/shard_map/ppermute | solution.py:10
  224.9 0.7 convert_multiply_fusion.4
  225.6 0.7 convert_multiply_fusion.2
  226.3 5.9 %all-to-all-done.6 = bf16[8,256,128]{2,1,0:T(8,128)(2,1)S(1)} async-done(((bf16[8,256,128]{2,1,0:T(8,128)(2,1)}), bf16[8,256,128]{2,1,0:T(8,128)(2,1)S(1)}, u32[]{:S(2)}, u32[]{:S(2)}) %all-to-all-start.6) | async-done | bytes 524320 | tf_op jit(solution)/shard_map/all_to_all | solution.py:15
  232.2 0.7 convert_reduce_fusion
  (139 shorter events, 8.6 us)
Async XLA Ops:
  7.2 23.5 %copy-start.39 = (s32[256,2]{0,1:T(2,128)S(1)}, s32[256,2]{0,1:T(2,128)}, u32[]{:S(2)}) copy-start(s32[256,2]{0,1:T(2,128)} %param.14) | copy-start | bytes 6148
  7.2 23.5 %copy-start.46 = (f32[256,2]{0,1:T(2,128)S(1)}, f32[256,2]{0,1:T(2,128)}, u32[]{:S(2)}) copy-start(f32[256,2]{0,1:T(2,128)} %param.15) | copy-start | bytes 6148
  7.2 81.7 %all-gather.10.cloned.1.call-start = ((), (), s32[]{:S(2)}) async-start(), calls=%async_computation.9 | async-start | bytes 2621440 | tf_op jit(solution)/shard_map/all_gather | solution.py:104
  7.3 23.8 %copy-start.42 = (f32[64]{0:T(128)}, f32[64]{0:T(128)S(1)}, u32[]{:S(2)}) copy-start(f32[64]{0:T(128)S(1)} %get-tuple-element.57) | copy-start | bytes 772
  7.3 42.7 %copy-start.44 = (f32[64]{0:T(128)}, f32[64]{0:T(128)S(1)}, u32[]{:S(2)}) copy-start(f32[64]{0:T(128)S(1)} %get-tuple-element.58) | copy-start | bytes 772
  30.7 64.5 %all-gather.12.cloned.1.call-start = ((), (), s32[]{:S(2)}) async-start(), calls=%async_computation.10 | async-start | bytes 2621440 | tf_op jit(solution)/shard_map/all_gather | solution.py:104
  50.0 57.8 %all-gather.8.cloned.1.call-start = ((), (), s32[]{:S(2)}) async-start(), calls=%async_computation.8 | async-start | bytes 2621440 | tf_op jit(solution)/shard_map/all_gather | solution.py:104
  50.1 24.0 %copy-start.34 = (bf16[256,128]{1,0:T(8,128)(2,1)S(1)}, bf16[256,128]{1,0:T(8,128)(2,1)}, u32[]{:S(2)}) copy-start(bf16[256,128]{1,0:T(8,128)(2,1)} %param.21) | copy-start | bytes 196612
  50.1 24.0 %copy-start.37 = (bf16[256,128]{1,0:T(8,128)(2,1)S(1)}, bf16[256,128]{1,0:T(8,128)(2,1)}, u32[]{:S(2)}) copy-start(bf16[256,128]{1,0:T(8,128)(2,1)} %param.20) | copy-start | bytes 196612
  50.4 27.7 %copy-start.47 = (f32[3,128]{1,0:T(4,128)S(1)}, f32[3,128]{1,0:T(4,128)}, u32[]{:S(2)}) copy-start(f32[3,128]{1,0:T(4,128)} %param.22) | copy-start | bytes 4612
  50.5 27.8 %copy-start.26 = (bf16[1,2048,256]{2,1,0:T(8,128)(2,1)S(1)}, bf16[1,2048,256]{2,1,0:T(8,128)(2,1)}, u32[]{:S(2)}) copy-start(bf16[1,2048,256]{2,1,0:T(8,128)(2,1)} %param.16) | copy-start | bytes 3145732
  70.4 17.7 %all-to-all-start.3 = ((bf16[8,64,512]{2,1,0:T(8,128)(2,1)}), bf16[8,64,512]{2,1,0:T(8,128)(2,1)S(1)}, u32[]{:S(2)}, u32[]{:S(2)}) async-start(bf16[8,64,512]{2,1,0:T(8,128)(2,1)} %bitcast.9), calls=%async_computation.3 | async-start | bytes 1048576 | tf_op jit(solution)/shard_map/all_to_all | solution.py:15
  74.0 51.4 %all-gather.6.cloned.1.call-start = ((), (), s32[]{:S(2)}) async-start(), calls=%async_computation.7 | async-start | bytes 2621440 | tf_op jit(solution)/shard_map/all_gather | solution.py:104
  74.1 6.7 %collective-permute-start.2 = (f32[2,128]{1,0:T(2,128)S(1)}, f32[2,128]{1,0:T(2,128)S(1)}, u32[]{:S(2)}, u32[]{:S(2)}) collective-permute-start(f32[2,128]{1,0:T(2,128)S(1)} %slice.75), channel_id=1, source_target_pairs={{0,4},{4,8},{8,12},{12,16},{16,20},{20,24},{24,28},{1,5},{5,9},{9,... | collective-permute-start | bytes 3080 | tf_op jit(solution)/shard_map/ppermute | solution.py:10
  78.2 2.6 %copy-start.40 = (f32[128]{0:T(128)}, f32[128]{0:T(128)S(1)}, u32[]{:S(2)}) copy-start(f32[128]{0:T(128)S(1)} %get-tuple-element.51) | copy-start | bytes 1540
  78.2 2.6 %copy-start.32 = (bf16[256,128]{1,0:T(8,128)(2,1)S(1)}, bf16[256,128]{1,0:T(8,128)(2,1)}, u32[]{:S(2)}) copy-start(bf16[256,128]{1,0:T(8,128)(2,1)} %param.19) | copy-start | bytes 196612
  88.9 3.5 %copy-start.1 = (bf16[512,2048]{1,0:T(8,128)(2,1)S(1)}, bf16[512,2048]{1,0:T(8,128)(2,1)}, u32[]{:S(2)}) copy-start(bf16[512,2048]{1,0:T(8,128)(2,1)} %all-gather.10.cloned.1.call-done) | copy-start | bytes 6291460
  95.2 3.1 %copy-start.13 = (bf16[512,256]{1,0:T(8,128)(2,1)S(1)}, bf16[512,256]{1,0:T(8,128)(2,1)}, u32[]{:S(2)}) copy-start(bf16[512,256]{1,0:T(8,128)(2,1)} %get-tuple-element.53) | copy-start | bytes 786436
  95.2 3.1 %copy-start.15 = (bf16[512,256]{1,0:T(8,128)(2,1)S(1)}, bf16[512,256]{1,0:T(8,128)(2,1)}, u32[]{:S(2)}) copy-start(bf16[512,256]{1,0:T(8,128)(2,1)} %get-tuple-element.54) | copy-start | bytes 786436
  100.8 56.5 %collective-permute-start.3 = (bf16[512,1024]{1,0:T(8,128)(2,1)}, bf16[512,1024]{1,0:T(8,128)(2,1)}, u32[]{:S(2)}, u32[]{:S(2)}) collective-permute-start(bf16[512,1024]{1,0:T(8,128)(2,1)} %add_convert_fusion), channel_id=1, source_target_pairs={{0,1},{1,0},{2,3},{3,2},{4,5},{5,4},{6,7},{7,6},{8,9},{9,8},{10,11... | collective-permute-start | bytes 3145736 | tf_op jit(solution)/shard_map/ppermute | solution.py:41
  104.7 2.3 copy-start.31
  107.8 3.7 %copy-start.4 = (bf16[512,2048]{1,0:T(8,128)(2,1)S(1)}, bf16[512,2048]{1,0:T(8,128)(2,1)}, u32[]{:S(2)}) copy-start(bf16[512,2048]{1,0:T(8,128)(2,1)} %all-gather.8.cloned.1.call-done) | copy-start | bytes 6291460
  107.8 3.7 %copy-start.27 = (bf16[1,2048,256]{2,1,0:T(8,128)(2,1)S(1)}, bf16[1,2048,256]{2,1,0:T(8,128)(2,1)}, u32[]{:S(2)}) copy-start(bf16[1,2048,256]{2,1,0:T(8,128)(2,1)} %param.17) | copy-start | bytes 3145732
  125.4 3.0 %copy-start.14 = (bf16[512,256]{1,0:T(8,128)(2,1)S(1)}, bf16[512,256]{1,0:T(8,128)(2,1)}, u32[]{:S(2)}) copy-start(bf16[512,256]{1,0:T(8,128)(2,1)} %get-tuple-element.53) | copy-start | bytes 786436
  125.4 3.1 %copy-start.16 = (bf16[512,256]{1,0:T(8,128)(2,1)S(1)}, bf16[512,256]{1,0:T(8,128)(2,1)}, u32[]{:S(2)}) copy-start(bf16[512,256]{1,0:T(8,128)(2,1)} %get-tuple-element.54) | copy-start | bytes 786436
  129.9 2.2 copy-start.10
  129.9 2.2 copy-start.12
  130.0 6.3 %collective-permute-start = (bf16[512,1024]{1,0:T(8,128)(2,1)S(1)}, bf16[512,1024]{1,0:T(8,128)(2,1)S(1)}, u32[]{:S(2)}, u32[]{:S(2)}) collective-permute-start(bf16[512,1024]{1,0:T(8,128)(2,1)S(1)} %add_convert_fusion.2), channel_id=1, source_target_pairs={{0,1},{1,0},{2,3},{3,2},{4,5},{5,4},{6,7},{7,6},{8,9},{9,8},{10,11... | collective-permute-start | bytes 3145736 | tf_op jit(solution)/shard_map/ppermute | solution.py:41
  134.5 2.4 copy-start.2
  136.5 2.2 copy-start.23
  136.5 2.2 copy-start.28
  136.5 2.2 copy-start.29
  136.5 14.1 %collective-permute-start.1 = (bf16[512,512]{1,0:T(8,128)(2,1)S(1)}, bf16[512,512]{1,0:T(8,128)(2,1)S(1)}, u32[]{:S(2)}, u32[]{:S(2)}) collective-permute-start(bf16[512,512]{1,0:T(8,128)(2,1)S(1)} %add_convert_fusion.7), channel_id=1, source_target_pairs={{0,2},{1,3},{2,0},{3,1},{4,6},{5,7},{6,4},{7,5},{8,10},{9,11},{10,... | collective-permute-start | bytes 1572872 | tf_op jit(solution)/shard_map/ppermute | solution.py:41
  140.6 16.6 %copy-start.8 = (bf16[512,1024]{1,0:T(8,128)(2,1)S(1)}, bf16[512,1024]{1,0:T(8,128)(2,1)}, u32[]{:S(2)}) copy-start(bf16[512,1024]{1,0:T(8,128)(2,1)} %add_convert_fusion.1) | copy-start | bytes 3145732
  151.7 21.8 %all-to-all-start.5 = ((bf16[8,64,512]{2,1,0:T(8,128)(2,1)}), bf16[8,64,512]{2,1,0:T(8,128)(2,1)S(1)}, u32[]{:S(2)}, u32[]{:S(2)}) async-start(bf16[8,64,512]{2,1,0:T(8,128)(2,1)} %bitcast.30), calls=%async_computation.5 | async-start | bytes 1048576 | tf_op jit(solution)/shard_map/all_to_all | solution.py:15
  157.2 22.1 %copy-start.45 = (f32[64]{0:T(128)S(1)}, f32[64]{0:T(128)}, u32[]{:S(2)}) copy-start(f32[64]{0:T(128)} %copy-done.44) | copy-start | bytes 772
  158.5 33.4 %copy-start.43 = (f32[64]{0:T(128)S(1)}, f32[64]{0:T(128)}, u32[]{:S(2)}) copy-start(f32[64]{0:T(128)} %copy-done.42) | copy-start | bytes 772
  158.5 13.0 %collective-permute-start.4 = (bf16[512,512]{1,0:T(8,128)(2,1)S(1)}, bf16[512,512]{1,0:T(8,128)(2,1)S(1)}, u32[]{:S(2)}, u32[]{:S(2)}) collective-permute-start(bf16[512,512]{1,0:T(8,128)(2,1)S(1)} %add_convert_fusion.5), channel_id=1, source_target_pairs={{0,2},{1,3},{2,0},{3,1},{4,6},{5,7},{6,4},{7,5},{8,10},{9,11},{10,... | collective-permute-start | bytes 1572872 | tf_op jit(solution)/shard_map/ppermute | solution.py:41
  173.5 18.4 %all-to-all-start.4 = ((bf16[8,64,512]{2,1,0:T(8,128)(2,1)}), bf16[8,64,512]{2,1,0:T(8,128)(2,1)S(1)}, u32[]{:S(2)}, u32[]{:S(2)}) async-start(bf16[8,64,512]{2,1,0:T(8,128)(2,1)} %bitcast.28), calls=%async_computation.4 | async-start | bytes 1048576 | tf_op jit(solution)/shard_map/all_to_all | solution.py:15
  179.3 29.7 %copy-start.36 = (bf16[256,128]{1,0:T(8,128)(2,1)S(1)}, bf16[256,128]{1,0:T(8,128)(2,1)}, u32[]{:S(2)}) copy-start(bf16[256,128]{1,0:T(8,128)(2,1)} %get-tuple-element.25) | copy-start | bytes 196612
  179.3 29.7 %all-gather.14.cloned.1.call-start = ((), (), s32[]{:S(2)}) async-start(), calls=%async_computation.11 | async-start | bytes 1310720 | tf_op jit(solution)/shard_map/all_gather | solution.py:154
  179.7 37.5 %copy-start.33 = (bf16[256,128]{1,0:T(8,128)(2,1)S(1)}, bf16[256,128]{1,0:T(8,128)(2,1)}, u32[]{:S(2)}) copy-start(bf16[256,128]{1,0:T(8,128)(2,1)} %param.19) | copy-start | bytes 196612
  194.0 30.9 %copy-start.38 = (bf16[256,128]{1,0:T(8,128)(2,1)S(1)}, bf16[256,128]{1,0:T(8,128)(2,1)}, u32[]{:S(2)}) copy-start(bf16[256,128]{1,0:T(8,128)(2,1)} %param.20) | copy-start | bytes 196612
  194.0 30.9 %copy-start.41 = (f32[128]{0:T(128)S(1)}, f32[128]{0:T(128)}, u32[]{:S(2)}) copy-start(f32[128]{0:T(128)} %copy-done.40) | copy-start | bytes 1540
  209.0 8.3 %copy-start.7 = (bf16[256,2048]{1,0:T(8,128)(2,1)S(1)}, bf16[256,2048]{1,0:T(8,128)(2,1)}, u32[]{:S(2)}) copy-start(bf16[256,2048]{1,0:T(8,128)(2,1)} %all-gather.14.cloned.1.call-done) | copy-start | bytes 3145732
  211.6 14.0 %copy-start.35 = (bf16[256,128]{1,0:T(8,128)(2,1)S(1)}, bf16[256,128]{1,0:T(8,128)(2,1)}, u32[]{:S(2)}) copy-start(bf16[256,128]{1,0:T(8,128)(2,1)} %param.21) | copy-start | bytes 196612
  211.6 20.5 %all-to-all-start.6 = ((bf16[8,256,128]{2,1,0:T(8,128)(2,1)}), bf16[8,256,128]{2,1,0:T(8,128)(2,1)S(1)}, u32[]{:S(2)}, u32[]{:S(2)}) async-start(bf16[8,256,128]{2,1,0:T(8,128)(2,1)} %bitcast.32), calls=%async_computation.6 | async-start | bytes 1048576 | tf_op jit(solution)/shard_map/all_to_all | solution.py:15
  219.4 5.5 %collective-permute-start.5 = (f32[2,128]{1,0:T(2,128)S(1)}, f32[2,128]{1,0:T(2,128)S(1)}, u32[]{:S(2)}, u32[]{:S(2)}) collective-permute-start(f32[2,128]{1,0:T(2,128)S(1)} %slice.82), channel_id=1, source_target_pairs={{4,0},{8,4},{12,8},{16,12},{20,16},{24,20},{28,24},{5,1},{9,5},{13... | collective-permute-start | bytes 3080 | tf_op jit(solution)/shard_map/ppermute | solution.py:10
  (15 other events, 22.9 us)
Sparse Core Ops, SparseCore 0:
  30.8 21.5 all-gather.9
  54.0 22.5 all-gather.11
  78.1 22.5 all-gather.7
  102.7 22.6 all-gather.5
  194.1 14.8 all-gather.13
